TPU v7x, 32 devices: a whole 2x2x4 slice. The times are simulated.
32 devices in a mesh: sp: 8 (over z, x), tp: 4 (over y, core).
Axes of the slice: x: 2, y: 2, z: 4, core: 2. Of those that a mesh axis runs over, the one named last changes fastest.
Arguments:
- x_in: bfloat16 [4096, 1024], P('sp', 'tp'), may hold values from -6 to 6
- gate_b: bfloat16 [4096, 1024], P('sp', 'tp'), may hold values from -6 to 6
- gate_c: bfloat16 [4096, 1024], P('sp', 'tp'), may hold values from -6 to 6
- conv_taps: bfloat16 [3, 1024], P(None, 'tp'), may hold values from -3.5 to 3.5
- out_proj: bfloat16 [1024, 2048], P('tp'), may hold values from -0.1875 to 0.1875
- mix_gain: bfloat16 [2048], replicated, may hold values from 0.099609375 to 1.8984375
- resid: bfloat16 [4096, 2048], P(('sp', 'tp')), may hold values from -6 to 6
- pre_gain: bfloat16 [2048], replicated, may hold values from 0.099609375 to 1.8984375
- expert_gate: bfloat16 [8, 2048, 512], P('sp'), may hold values from -0.125 to 0.125
- expert_up: bfloat16 [8, 2048, 512], P('sp'), may hold values from -0.125 to 0.125
- expert_down: bfloat16 [8, 512, 2048], P('sp'), may hold values from -7.1594562 to 7.1594562
- shared_gate: bfloat16 [2048, 256], replicated, may hold values from -0.125 to 0.125
- shared_up: bfloat16 [2048, 256], replicated, may hold values from -0.125 to 0.125
- shared_down: bfloat16 [256, 2048], replicated, may hold values from -10.125 to 10.125
- post_gain: bfloat16 [2048], replicated, may hold values from 0.099609375 to 1.8984375
- routes: int32 [4096, 4], P(('sp', 'tp')), may hold values from 0 to 7, all different within a row; in each aligned block of 128 rows (0 to 127, 128 to 255, ...) at most 96 rows name the same one
- route_weights: float32 [4096, 4], P(('sp', 'tp')), may hold values from 0.1 to 1
Outputs:
- layer_out: bfloat16 [4096, 2048], P(('sp', 'tp'))
Inputs may be any that keep to these rules, and one draw needn't show every extreme that they name: `routes`: each row names 4 different experts. Within the rows of one device (aligned blocks), no expert is named by more than 96 rows, and in some block one expert is named by exactly 96 rows.
All inputs are finite; a program needn't handle non-finite values.
Results may differ from a plain program's by a relative error of at most 0.007.
Values may be sent and summed in bfloat16 or wider, within the bound.
A program may use at most 128 MiB of HBM per device.

v0:
```python
import functools

import jax
import jax.numpy as jnp
from jax import lax
from jax.experimental import pallas as pl
from jax.experimental.pallas import tpu as pltpu

P = jax.sharding.PartitionSpec
MESH = pl.DeviceIdType.MESH
epsilon = 1e-06
PIECES = 4
HALVES = 2
DIRECT = 2


def layer_kernel(
    line,
    x_ref,
    gate_b_ref,
    gate_c_ref,
    taps_ref,
    resid_ref,
    gains_ref,
    routes_ref,
    weights_ref,
    proj_ref,
    eg_ref,
    eu_ref,
    ed_ref,
    sg_ref,
    su_ref,
    sd_ref,
    out_ref,
    edge_x,
    edge_c,
    mixed,
    conv,
    conv_near,
    proj,
    part_out,
    part_in,
    projected,
    resid1,
    w_gate,
    w_up,
    w_down,
    s_gate,
    s_up,
    s_down,
    blocks,
    sums,
    shared,
    from_low,
    from_high,
    outgoing,
    shares,
    hidden,
    load_sem,
    e_send,
    e_recv,
    p_send,
    p_recv,
    c_send,
    c_recv,
    f_send,
    f_recv,
    wx_send,
    wx_recv,
    wn_send,
    wn_recv,
    wf_send,
    wf_recv,
    wr_send,
    wr_recv,
    t_send,
    t_recv,
    gu_send,
    gu_recv,
    gd_send,
    gd_recv,
    ru_send,
    ru_recv,
    rd_send,
    rd_recv,
):
    sp = lax.axis_index("sp")
    tp = lax.axis_index("tp")
    sp_size = lax.axis_size("sp")
    tp_size = lax.axis_size("tp")
    z = sp // 2
    x = sp % 2
    last = line - 1
    mate = z * 2 + 1 - x
    near = (tp // 2) * 2 + 1 - tp % 2
    far = (tp + 2) % tp_size
    near_far = (near + 2) % tp_size
    rows, width = resid_ref.shape
    step_rows = rows // PIECES
    hid = w_gate.shape[2]
    shared_hid = s_gate.shape[1]

    barrier = pltpu.get_barrier_semaphore()
    for k in range(1, sp_size):
        pl.semaphore_signal(barrier, inc=1, device_id=((sp + k) % sp_size, tp), device_id_type=MESH)
    for k in range(1, tp_size):
        pl.semaphore_signal(barrier, inc=1, device_id=(sp, (tp + k) % tp_size), device_id_type=MESH)

    loads = [
        pltpu.make_async_copy(src, dst, load_sem.at[n])
        for n, (src, dst) in enumerate(
            (
                (eg_ref.at[0], w_gate.at[0]),
                (eu_ref.at[0], w_up.at[0]),
                (ed_ref.at[0], w_down.at[0]),
                (sg_ref, s_gate),
                (su_ref, s_up),
                (sd_ref, s_down),
                (proj_ref, proj.at[0]),
            )
        )
    ]
    loads[-1].start()
    for load in loads[:-1]:
        load.start()

    all_rows, channels = x_ref.shape
    reach = taps_ref.shape[0] - 1
    pad = edge_x.shape[0]
    mixed[pad:] = x_ref[...].astype(jnp.float32) * gate_c_ref[...].astype(jnp.float32)

    def edge_copy(n):
        source, landing = ((x_ref, edge_x), (gate_c_ref, edge_c))[n]
        return pltpu.make_async_remote_copy(
            src_ref=source.at[pl.ds(all_rows - pad, pad)],
            dst_ref=landing,
            send_sem=e_send.at[n],
            recv_sem=e_recv.at[n],
            device_id=((sp + 1) % sp_size, tp),
            device_id_type=MESH,
        )

    proj_copy = pltpu.make_async_remote_copy(
        src_ref=proj_ref,
        dst_ref=proj.at[1],
        send_sem=p_send.at[0],
        recv_sem=p_recv.at[0],
        device_id=(sp, near),
        device_id_type=MESH,
    )

    def block_rows(owner):
        return pl.ds(pl.multiple_of(owner * rows, rows), rows)

    def conv_copy(n):
        return pltpu.make_async_remote_copy(
            src_ref=conv.at[block_rows((near, near_far)[n])],
            dst_ref=conv_near.at[n],
            send_sem=c_send.at[n],
            recv_sem=c_recv.at[n],
            device_id=(sp, near),
            device_id_type=MESH,
        )

    part_cols = width // PIECES

    def part_copy(j):
        cols = pl.ds(pl.multiple_of(j * part_cols, part_cols), part_cols)
        return pltpu.make_async_remote_copy(
            src_ref=part_out.at[:, cols],
            dst_ref=part_in.at[:, cols],
            send_sem=f_send.at[j],
            recv_sem=f_recv.at[j],
            device_id=(sp, far),
            device_id_type=MESH,
        )

    pl.semaphore_wait(barrier, sp_size - 1 + tp_size - 1)

    @pl.when(sp < sp_size - 1)
    def _():
        edge_copy(0).start()
        edge_copy(1).start()

    proj_copy.start()

    pieces = []
    for ref, held in ((eg_ref, w_gate), (eu_ref, w_up), (ed_ref, w_down)):
        size = ref.shape[1] // tp_size // HALVES
        for h in range(HALVES):
            pieces.append((ref, held, size, h))

    def span(owner, n):
        _, _, size, h = pieces[n]
        return pl.ds(pl.multiple_of((owner * HALVES + h) * size, size), size)

    def hop(n, owner, target, send, recv, first=False):
        ref, held, _, _ = pieces[n]
        where = span(owner, n)
        return pltpu.make_async_remote_copy(
            src_ref=ref.at[0, where] if first else held.at[1, where],
            dst_ref=held.at[1, where],
            send_sem=send.at[n],
            recv_sem=recv.at[n],
            device_id=target,
            device_id_type=MESH,
        )

    def x_hop(n):
        return hop(n, tp, (mate, tp), wx_send, wx_recv, True)

    def near_hop(n, owner):
        return hop(n, owner, (sp, near), wn_send, wn_recv)

    def far_hop(n, owner):
        return hop(n, owner, (sp, far), wf_send, wf_recv)

    def direct_hop(n):
        return hop(n, far, (mate, tp), wf_send, wf_recv, True)

    def relay_hop(n, owner):
        return hop(n, owner, (sp, near), wr_send, wr_recv)

    count = len(pieces)

    def line_copy(source, landing, b, c, up, send, recv):
        part = pl.ds(pl.multiple_of(c * step_rows, step_rows), step_rows)
        return pltpu.make_async_remote_copy(
            src_ref=source.at[b, part],
            dst_ref=landing.at[b, part],
            send_sem=send.at[b, c],
            recv_sem=recv.at[b, c],
            device_id=((z + (1 if up else -1)) * 2 + x, tp),
            device_id_type=MESH,
        )

    def go_up(b, c):
        return line_copy(blocks, blocks, b, c, True, gu_send, gu_recv)

    def go_down(b, c):
        return line_copy(blocks, blocks, b, c, False, gd_send, gd_recv)

    def back_up(b, c):
        return line_copy(outgoing, from_low, b, c, True, ru_send, ru_recv)

    def back_down(b, c):
        return line_copy(outgoing, from_high, b, c, False, rd_send, rd_recv)

    def share_copy(k, source):
        return pltpu.make_async_remote_copy(
            src_ref=shares.at[source],
            dst_ref=shares.at[source],
            send_sem=t_send.at[k],
            recv_sem=t_recv.at[source],
            device_id=(((z + k) % line) * 2 + x, tp),
            device_id_type=MESH,
        )

    for n in range(count):
        x_hop(n).start()
    for n in range(count - DIRECT, count):
        direct_hop(n).start()

    lanes = lax.broadcasted_iota(jnp.int32, (rows, shares.shape[2]), 1)
    table = jnp.zeros((rows, shares.shape[2]), jnp.float32)
    for k in range(routes_ref.shape[1]):
        table += jnp.where(lanes == routes_ref[:, k : k + 1], weights_ref[:, k : k + 1], 0.0)
    shares[z] = table

    @pl.when(sp > 0)
    def _():
        edge_copy(0).wait_recv()
        edge_copy(1).wait_recv()
        mixed[:pad] = edge_x[...].astype(jnp.float32) * edge_c[...].astype(jnp.float32)

    @pl.when(sp == 0)
    def _():
        mixed[:pad] = jnp.zeros((pad, channels), jnp.float32)

    convolved = jnp.zeros((all_rows, channels), jnp.float32)
    for k in range(reach + 1):
        begin = pad - reach + k
        convolved += taps_ref[k : k + 1].astype(jnp.float32) * mixed[begin : begin + all_rows]
    conv[...] = (gate_b_ref[...].astype(jnp.float32) * convolved).astype(jnp.bfloat16)
    conv_copy(1).start()
    conv_copy(0).start()
    for k in range(1, line):
        share_copy(k, z).start()
    loads[-1].wait()
    proj_copy.wait_recv()

    def project(n, owner, cols):
        return jnp.dot(
            conv[block_rows(owner)], proj[0, :, cols], preferred_element_type=jnp.float32
        ) + jnp.dot(conv_near[n], proj[1, :, cols], preferred_element_type=jnp.float32)

    conv_copy(1).wait_recv()

    @pl.loop(0, PIECES)
    def _(j):
        cols = pl.ds(pl.multiple_of(j * part_cols, part_cols), part_cols)
        part_out[:, cols] = project(1, far, cols).astype(jnp.bfloat16)
        part_copy(j).start()

    conv_copy(0).wait_recv()

    @pl.loop(0, PIECES)
    def _(j):
        cols = pl.ds(pl.multiple_of(j * part_cols, part_cols), part_cols)
        projected[:, cols] = project(0, tp, cols)

    sums[...] = jnp.zeros_like(sums)

    def spread(n):
        x_hop(n).wait_recv()
        if n < count - DIRECT:
            far_hop(n, tp).start()
        near_hop(n, tp).start()

    for n in range(count // 2):
        spread(n)

    @pl.loop(0, PIECES)
    def _(j):
        cols = pl.ds(pl.multiple_of(j * part_cols, part_cols), part_cols)
        part_copy(j).wait_recv()
        projected[:, cols] += part_in[:, cols].astype(jnp.float32)

    def send_block(c):
        @pl.when(z < last)
        def _():
            go_up(z, c).start()

        @pl.when(z > 0)
        def _():
            go_down(z, c).start()

    for c in range(PIECES):
        part = pl.ds(c * step_rows, step_rows)
        block = projected[part]
        scale = lax.rsqrt(jnp.mean(block * block, axis=1, keepdims=True) + epsilon)
        mid = (
            resid_ref[part].astype(jnp.float32)
            + block * scale * gains_ref[0:1].astype(jnp.float32)
        ).astype(jnp.bfloat16)
        resid1[part] = mid
        wide = mid.astype(jnp.float32)
        normal = lax.rsqrt(jnp.mean(wide * wide, axis=1, keepdims=True) + epsilon)
        blocks[z, part] = (wide * normal * gains_ref[1:2].astype(jnp.float32)).astype(jnp.bfloat16)
        if c > 0:
            send_block(c - 1)
    send_block(PIECES - 1)

    def apply(b, i):
        expert = z * 2 + x + i * (1 - 2 * x)

        @pl.loop(0, hid // 256)
        def _(j):
            cols = pl.ds(pl.multiple_of(j * 256, 256), 256)
            gate = jnp.dot(blocks[b], w_gate[i, :, cols], preferred_element_type=jnp.float32)
            up = jnp.dot(blocks[b], w_up[i, :, cols], preferred_element_type=jnp.float32)
            hidden[:, cols] = (jax.nn.silu(gate) * up).astype(jnp.bfloat16)

        share = jnp.sum(jnp.where(lanes == expert, shares[b], 0.0), axis=1, keepdims=True)

        @pl.loop(0, width // 512)
        def _(j):
            cols = pl.ds(pl.multiple_of(j * 512, 512), 512)
            made = jnp.dot(hidden[...], w_down[i, :, cols], preferred_element_type=jnp.float32)
            made = made.astype(jnp.bfloat16).astype(jnp.float32)
            sums[b, :, cols] += jnp.where(share > 0.0, share * made, 0.0)

    def receive(t):
        @pl.loop(0, PIECES)
        def _(c):
            @pl.when(z - t >= 0)
            def _():
                go_up(z - t, c).wait_recv()

                @pl.when(z < last)
                def _():
                    go_up(z - t, c).start()

            @pl.when(z + t <= last)
            def _():
                go_down(z + t, c).wait_recv()

                @pl.when(z > 0)
                def _():
                    go_down(z + t, c).start()

    def apply_pair(t, i):
        @pl.loop(0, 2)
        def _(side):
            b = z - t + side * 2 * t

            @pl.when((b >= 0) & (b <= last))
            def _():
                apply(b, i)

    def give_back(t):
        p_up = t - z
        p_down = t - (last - z)
        b_up = (p_up + last) % last + 1
        b_down = last - ((p_down + last) % last + 1)
        send_up = (p_up >= 1) & (p_up <= last) & (b_up > z)
        send_down = (p_down >= 1) & (p_down <= last) & (b_down < z)

        @pl.loop(0, PIECES)
        def _(c):
            part = pl.ds(pl.multiple_of(c * step_rows, step_rows), step_rows)

            @pl.when(send_up)
            def _():
                @pl.when(z > 0)
                def _():
                    back_up(b_up, c).wait_recv()
                    sums[b_up, part] += from_low[b_up, part].astype(jnp.float32)

                outgoing[b_up, part] = sums[b_up, part].astype(jnp.bfloat16)
                back_up(b_up, c).start()

            @pl.when(send_down)
            def _():
                @pl.when(z < last)
                def _():
                    back_down(b_down, c).wait_recv()
                    sums[b_down, part] += from_high[b_down, part].astype(jnp.float32)

                outgoing[b_down, part] = sums[b_down, part].astype(jnp.bfloat16)
                back_down(b_down, c).start()

    for load in loads[:3]:
        load.wait()
    apply(z, 0)
    for load in loads[3:-1]:
        load.wait()
    s_g = jnp.dot(blocks[z], s_gate[...], preferred_element_type=jnp.float32)
    s_u = jnp.dot(blocks[z], s_up[...], preferred_element_type=jnp.float32)
    s_h = (jax.nn.silu(s_g) * s_u).astype(jnp.bfloat16)
    hidden[:, :shared_hid] = s_h

    @pl.loop(0, width // 512)
    def _(j):
        cols = pl.ds(pl.multiple_of(j * 512, 512), 512)
        shared[:, cols] = jnp.dot(
            hidden[:, :shared_hid], s_down[:, cols], preferred_element_type=jnp.float32
        )

    for n in range(count // 2, count):
        spread(n)
    receive(1)
    for k in range(1, line):
        share_copy(k, (z + k) % line).wait_recv()
    apply_pair(1, 0)

    def relay(n):
        far_hop(n, far).wait_recv()
        relay_hop(n, far).start()

    for n in range(2 * count // 3):
        relay(n)
    for t in range(2, last):
        receive(t)
        apply_pair(t, 0)
    for n in range(2 * count // 3, count):
        relay(n)
    for n in range(count):
        near_hop(n, near).wait_recv()
        relay_hop(n, near_far).wait_recv()

    @pl.loop(2, last)
    def _(t):
        apply_pair(t, 1)

    give_back(1)
    apply_pair(1, 1)
    receive(last)
    apply_pair(last, 0)
    apply_pair(last, 1)
    give_back(2)
    apply(z, 1)

    @pl.loop(3, 2 * last - 1)
    def _(t):
        give_back(t)

    @pl.loop(0, PIECES)
    def _(c):
        part = pl.ds(pl.multiple_of(c * step_rows, step_rows), step_rows)

        @pl.when(z > 0)
        def _():
            back_up(z, c).wait_recv()
            sums[z, part] += from_low[z, part].astype(jnp.float32)

        @pl.when(z < last)
        def _():
            back_down(z, c).wait_recv()
            sums[z, part] += from_high[z, part].astype(jnp.float32)

        branch = sums[z, part] + shared[part]
        factor = lax.rsqrt(jnp.mean(branch * branch, axis=1, keepdims=True) + epsilon)
        out_ref[part] = (
            resid1[part].astype(jnp.float32)
            + branch * factor * gains_ref[2:3].astype(jnp.float32)
        ).astype(jnp.bfloat16)

    @pl.when(sp < sp_size - 1)
    def _():
        edge_copy(0).wait_send()
        edge_copy(1).wait_send()

    proj_copy.wait_send()
    conv_copy(0).wait_send()
    conv_copy(1).wait_send()
    for j in range(PIECES):
        part_copy(j).wait_send()
    for n in range(count):
        x_hop(n).wait_send()
        near_hop(n, tp).wait_send()
        far_hop(n, tp).wait_send()
        relay_hop(n, far).wait_send()
    for k in range(1, line):
        share_copy(k, z).wait_send()

    @pl.loop(0, PIECES)
    def _(c):
        @pl.loop(0, line)
        def _(b):
            @pl.when((b <= z) & (z < last))
            def _():
                go_up(b, c).wait_send()

            @pl.when((b >= z) & (z > 0))
            def _():
                go_down(b, c).wait_send()

            @pl.when(b > z)
            def _():
                back_up(b, c).wait_send()

            @pl.when(b < z)
            def _():
                back_down(b, c).wait_send()


def fused_layer(
    x_in, gate_b, gate_c, conv_taps, out_proj, mix_gain, resid, pre_gain, expert_gate, expert_up,
    expert_down, shared_gate, shared_up, shared_down, post_gain, routes, route_weights,
):
    experts = lax.axis_size("sp")
    line = experts // 2
    all_rows, channels = x_in.shape
    rows, width = resid.shape
    hid = expert_gate.shape[2]
    shared_hid = shared_gate.shape[1]
    dma = pltpu.SemaphoreType.DMA
    count = 3 * HALVES
    bf, f32 = jnp.bfloat16, jnp.float32
    vmem = pl.BlockSpec(memory_space=pltpu.VMEM)
    hbm = pl.BlockSpec(memory_space=pltpu.HBM)
    lanes = 128 * (-(-experts // 128))
    pad = 16 * (-(-(conv_taps.shape[0] - 1) // 16))
    return pl.pallas_call(
        functools.partial(layer_kernel, line),
        out_shape=jax.ShapeDtypeStruct((rows, width), bf),
        in_specs=[vmem] * 8 + [hbm] * 7,
        out_specs=vmem,
        scratch_shapes=[
            pltpu.VMEM((pad, channels), bf),
            pltpu.VMEM((pad, channels), bf),
            pltpu.VMEM((pad + all_rows, channels), f32),
            pltpu.VMEM((all_rows, channels), bf),
            pltpu.VMEM((2, rows, channels), bf),
            pltpu.VMEM((2, channels, width), bf),
            pltpu.VMEM((rows, width), bf),
            pltpu.VMEM((rows, width), bf),
            pltpu.VMEM((rows, width), f32),
            pltpu.VMEM((rows, width), bf),
            pltpu.VMEM((2, width, hid), bf),
            pltpu.VMEM((2, width, hid), bf),
            pltpu.VMEM((2, hid, width), bf),
            pltpu.VMEM((width, shared_hid), bf),
            pltpu.VMEM((width, shared_hid), bf),
            pltpu.VMEM((shared_hid, width), bf),
            pltpu.VMEM((line, rows, width), bf),
            pltpu.VMEM((line, rows, width), f32),
            pltpu.VMEM((rows, width), f32),
            pltpu.VMEM((line, rows, width), bf),
            pltpu.VMEM((line, rows, width), bf),
            pltpu.VMEM((line, rows, width), bf),
            pltpu.VMEM((line, rows, lanes), f32),
            pltpu.VMEM((rows, max(hid, shared_hid)), bf),
            dma((7,)),
            dma((2,)),
            dma((2,)),
            dma((1,)),
            dma((1,)),
            dma((2,)),
            dma((2,)),
            dma((PIECES,)),
            dma((PIECES,)),
        ]
        + [dma((count,))] * 8
        + [dma((line,))] * 2
        + [dma((line, PIECES))] * 8,
        compiler_params=pltpu.CompilerParams(
            collective_id=0, has_side_effects=True, vmem_limit_bytes=60 * 1024 * 1024
        ),
    )(
        x_in, gate_b, gate_c, conv_taps, resid, jnp.stack([mix_gain, pre_gain, post_gain]),
        routes, route_weights, out_proj, expert_gate, expert_up, expert_down,
        shared_gate, shared_up, shared_down,
    )


def passed_along(shard, axis, by):
    size = lax.axis_size(axis)
    pairs = [(i, i + by) for i in range(size) if 0 <= i + by < size]
    return lax.ppermute(shard, axis, pairs)


def body(
    x_in,
    gate_b,
    gate_c,
    conv_taps,
    out_proj,
    mix_gain,
    resid,
    pre_gain,
    expert_gate,
    expert_up,
    expert_down,
    shared_gate,
    shared_up,
    shared_down,
    post_gain,
    routes,
    route_weights,
):
    group = lax.axis_size("sp")
    wide_slots = 3 * resid.shape[0] * routes.shape[1] // group
    if wide_slots > resid.shape[0] and group % 2 == 0 and lax.axis_size("tp") == 2 * 2:
        return fused_layer(
            x_in, gate_b, gate_c, conv_taps, out_proj, mix_gain, resid, pre_gain, expert_gate,
            expert_up, expert_down, shared_gate, shared_up, shared_down, post_gain, routes,
            route_weights,
        )
    row_count = x_in.shape[0]
    channels = x_in.shape[1]
    reach = conv_taps.shape[0] - 1
    edge_rows = jnp.concatenate([x_in[row_count - reach :], gate_c[row_count - reach :]], 1)
    arrived_edge = passed_along(edge_rows, "sp", 1)
    inputs = jnp.concatenate([arrived_edge[:, :channels], x_in], 0).astype(jnp.float32)
    gate_rows = jnp.concatenate([arrived_edge[:, channels:], gate_c], 0).astype(jnp.float32)
    mixed_in = inputs * gate_rows
    taps = conv_taps.astype(jnp.float32)
    convolved = jnp.zeros((row_count, channels), jnp.float32)
    for index in range(reach + 1):
        convolved = convolved + taps[index][None, :] * mixed_in[index : index + row_count]
    conv_out = (gate_b.astype(jnp.float32) * convolved).astype(jnp.bfloat16)
    width_all = out_proj.shape[1]
    full_rows = lax.all_to_all(conv_out, "tp", split_axis=0, concat_axis=1, tiled=True)
    projected = jnp.dot(
        full_rows,
        lax.all_gather(out_proj, "tp", axis=0, tiled=True),
        preferred_element_type=jnp.float32,
    )
    row_scale = lax.rsqrt(jnp.mean(projected * projected, axis=1, keepdims=True) + epsilon)
    resid1 = (
        resid.astype(jnp.float32) + projected * row_scale * mix_gain.astype(jnp.float32)
    ).astype(jnp.bfloat16)
    wide_resid = resid1.astype(jnp.float32)
    normed = (
        wide_resid
        * lax.rsqrt(jnp.mean(wide_resid * wide_resid, axis=1, keepdims=True) + epsilon)
        * pre_gain.astype(jnp.float32)
    ).astype(jnp.bfloat16)
    experts = lax.axis_size("sp")
    local_rows = resid.shape[0]
    top_count = routes.shape[1]
    capacity = 3 * local_rows * top_count // (2 * experts)
    flat_ids = routes.reshape(-1)
    onehot = (flat_ids[:, None] == jnp.arange(experts, dtype=jnp.int32)[None, :]).astype(jnp.int32)
    before = jnp.cumsum(onehot, axis=0) - onehot
    position = jnp.sum(before * onehot, axis=1)
    slot_index = flat_ids * capacity + position
    outgoing = (
        jnp.zeros((experts * capacity, width_all), jnp.bfloat16)
        .at[slot_index]
        .set(jnp.repeat(normed, top_count, axis=0))
    )
    received = lax.all_to_all(
        outgoing.reshape(experts, capacity, width_all),
        "sp",
        split_axis=0,
        concat_axis=0,
        tiled=True,
    )
    arrived = received.reshape(experts * capacity, width_all)
    gate_h = jnp.dot(arrived, expert_gate[0], preferred_element_type=jnp.float32)
    up_h = jnp.dot(arrived, expert_up[0], preferred_element_type=jnp.float32)
    hidden = (jax.nn.silu(gate_h) * up_h).astype(jnp.bfloat16)
    expert_out = jnp.dot(hidden, expert_down[0], preferred_element_type=jnp.float32).astype(
        jnp.bfloat16
    )
    returned = lax.all_to_all(
        expert_out.reshape(experts, capacity, width_all),
        "sp",
        split_axis=0,
        concat_axis=0,
        tiled=True,
    )
    returned = returned.reshape(experts * capacity, width_all)
    picked = returned[slot_index].astype(jnp.float32).reshape(local_rows, top_count, width_all)
    routed = jnp.einsum("tk,tkd->td", route_weights, picked)
    shared_g = jnp.dot(normed, shared_gate, preferred_element_type=jnp.float32)
    shared_u = jnp.dot(normed, shared_up, preferred_element_type=jnp.float32)
    shared_hidden = (jax.nn.silu(shared_g) * shared_u).astype(jnp.bfloat16)
    shared_out = jnp.dot(shared_hidden, shared_down, preferred_element_type=jnp.float32)
    branch = routed + shared_out
    factor = lax.rsqrt(jnp.mean(branch * branch, axis=1, keepdims=True) + epsilon)
    return (wide_resid + branch * factor * post_gain.astype(jnp.float32)[None, :]).astype(
        jnp.bfloat16
    )


def solution(mesh):
    return jax.shard_map(
        body,
        mesh=mesh,
        in_specs=(
            P("sp", "tp"),
            P("sp", "tp"),
            P("sp", "tp"),
            P(None, "tp"),
            P("tp", None),
            P(),
            P(("sp", "tp"), None),
            P(),
            P("sp", None, None),
            P("sp", None, None),
            P("sp", None, None),
            P(),
            P(),
            P(),
            P(),
            P(("sp", "tp"), None),
            P(("sp", "tp"), None),
        ),
        out_specs=P(("sp", "tp"), None),
        check_vma=False,
    )
```

profile of v0, /device:TPU:0, one launch (start us, length us, event | category | flops | bytes accessed | tf_op | source)
XLA Modules:
  0.0 107.4 jit_solution(3705305805073913260)
XLA Ops:
  0.0 0.7 stack.12
  0.7 0.7 stack.13
  1.4 0.7 stack.14
  2.1 0.6 pad_maximum_fusion.gains_ref
  2.7 1.4 %copy.18.routes_ref = s32[128,4]{1,0:T(8,128)} copy(s32[128,4]{0,1:T(4,128)} %param.32) | data formatting | bytes 4096 | tf_op args[15]
  4.1 1.4 %copy.19.weights_ref = f32[128,4]{1,0:T(8,128)} copy(f32[128,4]{0,1:T(4,128)} %param.33) | data formatting | bytes 4096 | tf_op args[16]
  5.5 100.0 %shard_map.163 = bf16[128,2048]{1,0:T(8,128)(2,1)} custom-call(bf16[512,256]{1,0:T(8,128)(2,1)} %x_ref.1, bf16[512,256]{1,0:T(8,128)(2,1)} %gate_b_ref.1, bf16[512,256]{1,0:T(8,128)(2,1)} %gate_c_ref.1, bf16[3,256]{1,0:T(4,128)(2,1)} %taps_ref.1, bf16[128,2048]{1,0:T(8,128)(2,1)} %resid_ref.1, bf16[3,2048]{1,0:T(4,128)(2,1)} %pad_maximum_fusion.gains_ref, ...), custom_call_target="tpu_custom_call" | custom-call | tf_op jit(solution)/shard_map/pallas_call | solution.py:565
  105.6 1.9 %copy.21 = bf16[128,2048]{1,0:T(8,128)(2,1)} copy(bf16[128,2048]{1,0:T(8,128)(2,1)} %shard_map.163) | data formatting | bytes 1048576
where the time goes:
time: 109 us; the launch traced here: 107 us
  Pallas kernels  100 us (92%)
  local copies, waits for them, and re-layouts  6.78 us (6%)
    pallas_call x1, Pallas kernels, fused_layer(): pl.pallas_call(functools.partial(layer_kernel, line), out_shape=jax.Shape...  100 us
    unnamed x3, local copies, waits for them, and re-layouts  4.7 us

commit v1 on v0

--- a/solution.py
+++ b/solution.py
@@ -21,7 +21,9 @@
     gate_c_ref,
     taps_ref,
     resid_ref,
-    gains_ref,
+    mix_ref,
+    pre_ref,
+    post_ref,
     routes_ref,
     weights_ref,
     proj_ref,
@@ -262,10 +264,11 @@
         direct_hop(n).start()
 
     lanes = lax.broadcasted_iota(jnp.int32, (rows, shares.shape[2]), 1)
-    table = jnp.zeros((rows, shares.shape[2]), jnp.float32)
-    for k in range(routes_ref.shape[1]):
-        table += jnp.where(lanes == routes_ref[:, k : k + 1], weights_ref[:, k : k + 1], 0.0)
-    shares[z] = table
+    names = lax.broadcasted_iota(jnp.int32, (shares.shape[2], rows), 0)
+    table = jnp.zeros((shares.shape[2], rows), jnp.float32)
+    for k in range(routes_ref.shape[0]):
+        table += jnp.where(names == routes_ref[k : k + 1], weights_ref[k : k + 1], 0.0)
+    shares[z] = table.T
 
     @pl.when(sp > 0)
     def _():
@@ -341,12 +344,12 @@
         scale = lax.rsqrt(jnp.mean(block * block, axis=1, keepdims=True) + epsilon)
         mid = (
             resid_ref[part].astype(jnp.float32)
-            + block * scale * gains_ref[0:1].astype(jnp.float32)
+            + block * scale * mix_ref[...].astype(jnp.float32).reshape(1, width)
         ).astype(jnp.bfloat16)
         resid1[part] = mid
         wide = mid.astype(jnp.float32)
         normal = lax.rsqrt(jnp.mean(wide * wide, axis=1, keepdims=True) + epsilon)
-        blocks[z, part] = (wide * normal * gains_ref[1:2].astype(jnp.float32)).astype(jnp.bfloat16)
+        blocks[z, part] = (wide * normal * pre_ref[...].astype(jnp.float32).reshape(1, width)).astype(jnp.bfloat16)
         if c > 0:
             send_block(c - 1)
     send_block(PIECES - 1)
@@ -503,7 +506,7 @@
         factor = lax.rsqrt(jnp.mean(branch * branch, axis=1, keepdims=True) + epsilon)
         out_ref[part] = (
             resid1[part].astype(jnp.float32)
-            + branch * factor * gains_ref[2:3].astype(jnp.float32)
+            + branch * factor * post_ref[...].astype(jnp.float32).reshape(1, width)
         ).astype(jnp.bfloat16)
 
     @pl.when(sp < sp_size - 1)
@@ -565,7 +568,7 @@
     return pl.pallas_call(
         functools.partial(layer_kernel, line),
         out_shape=jax.ShapeDtypeStruct((rows, width), bf),
-        in_specs=[vmem] * 8 + [hbm] * 7,
+        in_specs=[vmem] * 10 + [hbm] * 7,
         out_specs=vmem,
         scratch_shapes=[
             pltpu.VMEM((pad, channels), bf),
@@ -609,8 +612,8 @@
             collective_id=0, has_side_effects=True, vmem_limit_bytes=60 * 1024 * 1024
         ),
     )(
-        x_in, gate_b, gate_c, conv_taps, resid, jnp.stack([mix_gain, pre_gain, post_gain]),
-        routes, route_weights, out_proj, expert_gate, expert_up, expert_down,
+        x_in, gate_b, gate_c, conv_taps, resid, mix_gain, pre_gain, post_gain,
+        routes.T, route_weights.T, out_proj, expert_gate, expert_up, expert_down,
         shared_gate, shared_up, shared_down,
     )
 

time: 109 us -> 103 us (0.945)
  local copies, waits for them, and re-layouts: 6.78 us -> 1.88 us
    unnamed x3 -> x1, local copies, waits for them, and re-layouts: 4.7 us -> 1.88 us
    another operation x3 -> x0, local copies, waits for them, and re-layouts: 2.08 us -> none  [fused_layer(): jnp.stack([mix_gain, pre_gain, post_gain])]
where the time goes in v1:
time: 103 us; the launch traced here: 102 us
  Pallas kernels  100 us (97%)
  local copies, waits for them, and re-layouts  1.88 us (2%)
    pallas_call x1, Pallas kernels, fused_layer(): pl.pallas_call(functools.partial(layer_kernel, line), out_shape=jax.Shape...  100 us

profile of v1, /device:TPU:0, one launch (start us, length us, event | category | flops | bytes accessed | tf_op | source)
XLA Modules:
  0.0 101.9 jit_solution(3056184321861350889)
XLA Ops:
  0.0 100.0 %shard_map.163 = bf16[128,2048]{1,0:T(8,128)(2,1)} custom-call(bf16[512,256]{1,0:T(8,128)(2,1)} %x_ref.1, bf16[512,256]{1,0:T(8,128)(2,1)} %gate_b_ref.1, bf16[512,256]{1,0:T(8,128)(2,1)} %gate_c_ref.1, bf16[3,256]{1,0:T(4,128)(2,1)} %taps_ref.1, bf16[128,2048]{1,0:T(8,128)(2,1)} %resid_ref.1, bf16[2048]{0:T(1024)(128)(2,1)} %mix_ref.1, ...), custom_call_target="tpu_custom_call" | custom-call | tf_op jit(solution)/shard_map/pallas_call | solution.py:568
  100.0 1.9 %copy.19 = bf16[128,2048]{1,0:T(8,128)(2,1)} copy(bf16[128,2048]{1,0:T(8,128)(2,1)} %shard_map.163) | data formatting | bytes 1048576

commit v2 on v1

v2 whole, which is shorter than its diff:
```python
import functools

import jax
import jax.numpy as jnp
from jax import lax
from jax.experimental import pallas as pl
from jax.experimental.pallas import tpu as pltpu

P = jax.sharding.PartitionSpec
MESH = pl.DeviceIdType.MESH
epsilon = 1e-06
PIECES = 4
HALVES = 2
DIRECT = (3, 7)
TABLE = HALVES


def layer_kernel(
    line,
    x_hbm,
    gate_b_hbm,
    gate_c_hbm,
    taps_hbm,
    resid_hbm,
    mix_hbm,
    pre_hbm,
    post_hbm,
    routes_hbm,
    weights_hbm,
    proj_ref,
    eg_ref,
    eu_ref,
    ed_ref,
    sg_ref,
    su_ref,
    sd_ref,
    out_ref,
    x_ref,
    gate_b_ref,
    gate_c_ref,
    taps_ref,
    resid_ref,
    mix_ref,
    pre_ref,
    post_ref,
    routes_ref,
    weights_ref,
    edge_x,
    edge_c,
    mixed,
    conv,
    conv_near,
    proj,
    part_out,
    part_in,
    projected,
    resid1,
    w_gate,
    w_up,
    w_down,
    s_gate,
    s_up,
    s_down,
    blocks,
    shares,
    hidden,
    shared_hidden,
    branch,
    outgoing,
    from_out,
    from_in,
    load_sem,
    e_send,
    e_recv,
    p_send,
    p_recv,
    c_send,
    c_recv,
    f_send,
    f_recv,
    wx_send,
    wx_recv,
    wn_send,
    wn_recv,
    wf_send,
    wf_recv,
    wr_send,
    wr_recv,
    gi_send,
    go_send,
    gi_recv,
    go_recv,
    ri_send,
    ro_send,
    ri_recv,
    ro_recv,
):
    sp = lax.axis_index("sp")
    tp = lax.axis_index("tp")
    sp_size = lax.axis_size("sp")
    tp_size = lax.axis_size("tp")
    z = sp // 2
    x = sp % 2
    last = line - 1
    mate = z * 2 + 1 - x
    near = (tp // 2) * 2 + 1 - tp % 2
    far = (tp + 2) % tp_size
    near_far = (near + 2) % tp_size
    upper = z // (line // 2)
    inward_step = 1 - 2 * upper
    level = upper * last + inward_step * z
    inward = ((z + inward_step) * 2 + x, tp)
    outward = ((z - inward_step) * 2 + x, tp)

    def rel(k):
        return upper * last + inward_step * k

    rows, width = resid_ref.shape
    half_rows = rows // HALVES
    hid = w_gate.shape[2]
    shared_hid = s_gate.shape[1]
    part_cols = width // PIECES

    barrier = pltpu.get_barrier_semaphore()

    def greet(device):
        pl.semaphore_signal(barrier, inc=1, device_id=device, device_id_type=MESH)

    greet((mate, tp))
    greet((sp, near))
    greet((sp, far))

    @pl.when(z > 0)
    def _():
        greet((sp - 2, tp))

    @pl.when(z < last)
    def _():
        greet((sp + 2, tp))

    @pl.when((x == 1) & (z < last))
    def _():
        greet((sp + 1, tp))

    @pl.when((x == 0) & (z > 0))
    def _():
        greet((sp - 1, tp))

    pairs = (
        (x_hbm, x_ref),
        (gate_c_hbm, gate_c_ref),
        (proj_ref, proj.at[0]),
        (gate_b_hbm, gate_b_ref),
        (taps_hbm, taps_ref),
        (routes_hbm, routes_ref),
        (weights_hbm, weights_ref),
        (resid_hbm, resid_ref),
        (mix_hbm, mix_ref),
        (pre_hbm, pre_ref),
        (eg_ref.at[0], w_gate.at[0]),
        (eu_ref.at[0], w_up.at[0]),
        (sg_ref, s_gate),
        (su_ref, s_up),
        (ed_ref.at[0], w_down.at[pl.ds(0, hid)]),
        (sd_ref, s_down),
        (post_hbm, post_ref),
    )
    loads = [pltpu.make_async_copy(src, dst, load_sem.at[n]) for n, (src, dst) in enumerate(pairs)]
    for load in loads:
        load.start()

    all_rows, channels = x_ref.shape
    reach = taps_ref.shape[0] - 1
    pad = edge_x.shape[0]

    def edge_copy(n):
        source, landing = ((x_ref, edge_x), (gate_c_ref, edge_c))[n]
        return pltpu.make_async_remote_copy(
            src_ref=source.at[pl.ds(all_rows - pad, pad)],
            dst_ref=landing,
            send_sem=e_send.at[n],
            recv_sem=e_recv.at[n],
            device_id=((sp + 1) % sp_size, tp),
            device_id_type=MESH,
        )

    proj_copy = pltpu.make_async_remote_copy(
        src_ref=proj.at[0],
        dst_ref=proj.at[1],
        send_sem=p_send.at[0],
        recv_sem=p_recv.at[0],
        device_id=(sp, near),
        device_id_type=MESH,
    )

    def block_rows(owner):
        return pl.ds(pl.multiple_of(owner * rows, rows), rows)

    def conv_copy(n):
        return pltpu.make_async_remote_copy(
            src_ref=conv.at[block_rows((near, near_far)[n])],
            dst_ref=conv_near.at[n],
            send_sem=c_send.at[n],
            recv_sem=c_recv.at[n],
            device_id=(sp, near),
            device_id_type=MESH,
        )

    def chunk(j):
        return pl.ds(pl.multiple_of(j * part_cols, part_cols), part_cols)

    def half(r):
        return pl.ds(r * half_rows, half_rows)

    def part_copy(j):
        return pltpu.make_async_remote_copy(
            src_ref=part_out.at[:, chunk(j)],
            dst_ref=part_in.at[:, chunk(j)],
            send_sem=f_send.at[j],
            recv_sem=f_recv.at[j],
            device_id=(sp, far),
            device_id_type=MESH,
        )

    pieces = []
    for ref, held in ((eg_ref, w_gate), (eu_ref, w_up)):
        for h in range(HALVES):
            pieces.append((ref, held, h))
    for j in range(PIECES):
        pieces.append((ed_ref, w_down, j))
    count = len(pieces)

    def cut(n, owner):
        ref, held, h = pieces[n]
        if held is w_down:
            size = hid // tp_size
            begin = pl.multiple_of(owner * size, size)
            return (
                ref.at[0, pl.ds(begin, size), chunk(h)],
                held.at[pl.ds(pl.multiple_of(hid + begin, size), size), chunk(h)],
            )
        size = ref.shape[1] // tp_size // HALVES
        where = pl.ds(pl.multiple_of((owner * HALVES + h) * size, size), size)
        return ref.at[0, where], held.at[1, where]

    def hop(n, owner, target, send, recv, first=False):
        source, landing = cut(n, owner)
        return pltpu.make_async_remote_copy(
            src_ref=source if first else landing,
            dst_ref=landing,
            send_sem=send.at[n],
            recv_sem=recv.at[n],
            device_id=target,
            device_id_type=MESH,
        )

    def x_hop(n):
        return hop(n, tp, (mate, tp), wx_send, wx_recv, True)

    def near_hop(n, owner):
        return hop(n, owner, (sp, near), wn_send, wn_recv)

    def far_hop(n, owner):
        return hop(n, owner, (sp, far), wf_send, wf_recv)

    def direct_hop(n):
        return hop(n, far, (mate, tp), wf_send, wf_recv, True)

    def relay_hop(n, owner):
        return hop(n, owner, (sp, near), wr_send, wr_recv)

    def spread(n):
        with jax.named_scope("w_x"):
            x_hop(n).wait_recv()
        if n not in DIRECT:
            far_hop(n, tp).start()
        near_hop(n, tp).start()

    def relay(n):
        with jax.named_scope("w_far"):
            far_hop(n, far).wait_recv()
        relay_hop(n, far).start()

    def ready(n):
        with jax.named_scope("w_ready"):
            near_hop(n, near).wait_recv()
            relay_hop(n, near_far).wait_recv()

    def block_copy(b, r, target, send, recv):
        ref = shares.at[b] if r == TABLE else blocks.at[b, half(r)]
        return pltpu.make_async_remote_copy(
            src_ref=ref,
            dst_ref=ref,
            send_sem=send.at[b, r],
            recv_sem=recv.at[b, r],
            device_id=target,
            device_id_type=MESH,
        )

    def edge_in(b, r):
        return block_copy(b, r, inward, gi_send, go_recv)

    def mid_in(b, r):
        return block_copy(b, r, inward, gi_send, gi_recv)

    def mid_out(b, r):
        return block_copy(b, r, outward, go_send, gi_recv)

    def got_in(b, r):
        with jax.named_scope("w_gi"):
            block_copy(b, r, inward, gi_send, gi_recv).wait_recv()

    def got_out(b, r):
        with jax.named_scope("w_go"):
            block_copy(b, r, outward, go_send, go_recv).wait_recv()

    def sum_copy(b, r, j, landing, target, send, recv):
        return pltpu.make_async_remote_copy(
            src_ref=outgoing.at[b, half(r), chunk(j)],
            dst_ref=landing.at[b, half(r), chunk(j)],
            send_sem=send.at[b, r, j],
            recv_sem=recv.at[b, r, j],
            device_id=target,
            device_id_type=MESH,
        )

    def edge_give(b, r, j):
        return sum_copy(b, r, j, from_out, inward, ri_send, ro_recv)

    def mid_give_in(b, r, j):
        return sum_copy(b, r, j, from_in, inward, ri_send, ri_recv)

    def mid_give_out(b, r, j):
        return sum_copy(b, r, j, from_in, outward, ro_send, ri_recv)

    def sum_in(b, r, j):
        with jax.named_scope("w_ri"):
            sum_copy(b, r, j, from_in, inward, ri_send, ri_recv).wait_recv()

    def sum_out(b, r, j):
        with jax.named_scope("w_ro"):
            sum_copy(b, r, j, from_out, outward, ro_send, ro_recv).wait_recv()

    with jax.named_scope("w_barrier"):
        met = 3 + jnp.where(z > 0, 1, 0) + jnp.where(z < last, 1, 0)
        met += jnp.where(jnp.where(x == 1, z < last, z > 0), 1, 0)
        pl.semaphore_wait(barrier, met)

    for n in range(count):
        x_hop(n).start()
        if n in DIRECT:
            direct_hop(n).start()

    loads[0].wait()
    loads[1].wait()

    @pl.when(sp < sp_size - 1)
    def _():
        edge_copy(0).start()
        edge_copy(1).start()

    loads[2].wait()
    proj_copy.start()
    mixed[pad:] = x_ref[...].astype(jnp.float32) * gate_c_ref[...].astype(jnp.float32)
    loads[3].wait()
    loads[4].wait()

    with jax.named_scope("w_edge"):

        @pl.when(sp > 0)
        def _():
            edge_copy(0).wait_recv()
            edge_copy(1).wait_recv()
            mixed[:pad] = edge_x[...].astype(jnp.float32) * edge_c[...].astype(jnp.float32)

        @pl.when(sp == 0)
        def _():
            mixed[:pad] = jnp.zeros((pad, channels), jnp.float32)

    convolved = jnp.zeros((all_rows, channels), jnp.float32)
    for k in range(reach + 1):
        begin = pad - reach + k
        convolved += taps_ref[k : k + 1].astype(jnp.float32) * mixed[begin : begin + all_rows]
    conv[...] = (gate_b_ref[...].astype(jnp.float32) * convolved).astype(jnp.bfloat16)
    conv_copy(1).start()
    conv_copy(0).start()

    def project(n, owner, cols):
        return jnp.dot(
            conv[block_rows(owner)], proj[0, :, cols], preferred_element_type=jnp.float32
        ) + jnp.dot(conv_near[n], proj[1, :, cols], preferred_element_type=jnp.float32)

    with jax.named_scope("w_conv"):
        proj_copy.wait_recv()
        conv_copy(1).wait_recv()

    @pl.loop(0, PIECES)
    def _(j):
        part_out[:, chunk(j)] = project(1, far, chunk(j)).astype(jnp.bfloat16)
        part_copy(j).start()

    loads[5].wait()
    loads[6].wait()
    lanes = lax.broadcasted_iota(jnp.int32, (rows, shares.shape[2]), 1)
    names = lax.broadcasted_iota(jnp.int32, (shares.shape[2], rows), 0)
    table = jnp.zeros((shares.shape[2], rows), jnp.float32)
    for k in range(routes_ref.shape[0]):
        table += jnp.where(names == routes_ref[k : k + 1], weights_ref[k : k + 1], 0.0)
    shares[z] = table.T

    own = z

    @pl.when(level == 0)
    def _():
        edge_in(own, TABLE).start()

    @pl.when(level == 1)
    def _():
        mid_in(own, TABLE).start()
        mid_out(own, TABLE).start()

    conv_copy(0).wait_recv()

    @pl.loop(0, PIECES)
    def _(j):
        projected[:, chunk(j)] = project(0, tp, chunk(j))

    spread(0)
    spread(1)
    for load in loads[7:10]:
        load.wait()

    with jax.named_scope("w_part"):

        @pl.loop(0, PIECES)
        def _(j):
            part_copy(j).wait_recv()
            projected[:, chunk(j)] += part_in[:, chunk(j)].astype(jnp.float32)

    with jax.named_scope("norm"):
        for r in range(HALVES):
            part = half(r)
            block = projected[part]
            scale = lax.rsqrt(jnp.mean(block * block, axis=1, keepdims=True) + epsilon)
            mid = (
                resid_ref[part].astype(jnp.float32)
                + block * scale * mix_ref[...].astype(jnp.float32).reshape(1, width)
            ).astype(jnp.bfloat16)
            resid1[part] = mid
            wide = mid.astype(jnp.float32)
            normal = lax.rsqrt(jnp.mean(wide * wide, axis=1, keepdims=True) + epsilon)
            blocks[own, part] = (
                wide * normal * pre_ref[...].astype(jnp.float32).reshape(1, width)
            ).astype(jnp.bfloat16)

            @pl.when(level == 0)
            def _():
                edge_in(own, r).start()

            @pl.when(level == 1)
            def _():
                mid_in(own, r).start()
                mid_out(own, r).start()

    spread(2)

    def hide(b, begin, size, e):
        part = pl.ds(begin, size)
        expert = z * 2 + x + e * (1 - 2 * x)
        share = jnp.sum(
            jnp.where(lanes[:size] == expert, shares[b, part], 0.0), axis=1, keepdims=True
        )

        @pl.loop(0, hid // 256)
        def _(j):
            cols = pl.ds(pl.multiple_of(j * 256, 256), 256)
            gate = jnp.dot(blocks[b, part], w_gate[e, :, cols], preferred_element_type=jnp.float32)
            up = jnp.dot(blocks[b, part], w_up[e, :, cols], preferred_element_type=jnp.float32)
            kept = pl.ds(pl.multiple_of(e * hid + j * 256, 256), 256)
            hidden[b, part, kept] = (jax.nn.silu(gate) * up * share).astype(jnp.bfloat16)

    def hide_all(b, e):
        hide(b, 0, rows, e)

    def hide_half(b, r):
        hide(b, r * half_rows, half_rows, 0)
        hide(b, r * half_rows, half_rows, 1)

    def down(b, part, j):
        return jnp.dot(
            hidden[b, part], w_down[:, chunk(j)], preferred_element_type=jnp.float32
        )

    def give(b, r, j, arrived, send):
        made = down(b, half(r), j)
        if arrived is not None:
            made += arrived[b, half(r), chunk(j)].astype(jnp.float32)
        outgoing[b, half(r), chunk(j)] = made.astype(jnp.bfloat16)
        send(b, r, j).start()

    def shared_up_to_hidden():
        s_g = jnp.dot(blocks[own], s_gate[...], preferred_element_type=jnp.float32)
        s_u = jnp.dot(blocks[own], s_up[...], preferred_element_type=jnp.float32)
        shared_hidden[...] = (jax.nn.silu(s_g) * s_u).astype(jnp.bfloat16)

    def own_branch():
        @pl.loop(0, PIECES)
        def _(j):
            branch[:, chunk(j)] = down(own, pl.ds(0, rows), j) + jnp.dot(
                shared_hidden[...], s_down[:, chunk(j)], preferred_element_type=jnp.float32
            )

    def yield_out(part, total):
        factor = lax.rsqrt(jnp.mean(total * total, axis=1, keepdims=True) + epsilon)
        out_ref[part] = (
            resid1[part].astype(jnp.float32)
            + total * factor * post_ref[...].astype(jnp.float32).reshape(1, width)
        ).astype(jnp.bfloat16)

    for load in loads[10:14]:
        load.wait()
    hide_all(own, 0)
    shared_up_to_hidden()
    relay(0)
    spread(3)
    for load in loads[14:]:
        load.wait()

    @pl.when(level == 0)
    def _():
        b1, b2, b3 = rel(1), rel(2), rel(3)
        got_in(b1, TABLE)
        got_in(b1, 0)
        hide(b1, 0, half_rows, 0)
        relay(1)
        relay(3)
        got_in(b1, 1)
        hide(b1, half_rows, half_rows, 0)
        spread(4)
        relay(2)
        spread(5)
        got_in(b2, TABLE)
        got_in(b3, TABLE)
        for n in range(4):
            ready(n)
        hide_all(b1, 1)
        hide_all(own, 1)
        relay(4)
        spread(6)
        got_in(b2, 0)
        hide_half(b2, 0)
        ready(4)
        for r in range(HALVES):
            give(b1, r, 0, None, edge_give)
        give(b2, 0, 0, None, edge_give)
        relay(5)
        spread(7)
        ready(5)
        give(b2, 0, 1, None, edge_give)
        for r in range(HALVES):
            give(b1, r, 1, None, edge_give)
        relay(6)
        relay(7)
        got_in(b2, 1)
        hide_half(b2, 1)

        @pl.loop(0, 2)
        def _(j):
            give(b2, 1, j, None, edge_give)

        ready(6)
        ready(7)

        @pl.loop(2, PIECES)
        def _(j):
            for r in range(HALVES):
                give(b2, r, j, None, edge_give)

        own_branch()
        for r in range(HALVES):
            got_in(b3, r)
            hide_half(b3, r)

            @pl.loop(0, PIECES)
            def _(j):
                give(b3, r, j, None, edge_give)

        @pl.loop(2, PIECES)
        def _(j):
            for r in range(HALVES):
                give(b1, r, j, None, edge_give)

        for r in range(HALVES):

            @pl.loop(0, PIECES)
            def _(j):
                sum_in(own, r, j)

            total = branch[half(r)] + from_in[own, half(r)].astype(jnp.float32)
            yield_out(half(r), total)

        for r in range(HALVES + 1):
            edge_in(own, r).wait_send()

        @pl.loop(0, PIECES)
        def _(j):
            for b in (b1, b2, b3):
                for r in range(HALVES):
                    edge_give(b, r, j).wait_send()

    @pl.when(level == 1)
    def _():
        b0, b2, b3 = rel(0), rel(2), rel(3)

        def pass_in(r):
            got_out(b0, r)
            mid_in(b0, r).start()

        def pass_out(b, r):
            got_in(b, r)
            mid_out(b, r).start()

        pass_in(TABLE)
        pass_out(b2, TABLE)
        pass_in(0)
        pass_out(b2, 0)
        pass_out(b3, TABLE)
        relay(1)
        relay(3)
        pass_in(1)
        pass_out(b2, 1)
        hide_all(b0, 0)
        spread(4)
        hide_all(b2, 0)
        relay(2)
        spread(5)
        for n in range(4):
            ready(n)
        hide_all(b2, 1)
        relay(4)
        spread(6)
        hide_all(own, 1)
        pass_out(b3, 0)
        relay(5)
        spread(7)
        hide_all(b0, 1)
        relay(6)
        relay(7)
        pass_out(b3, 1)
        hide_all(b3, 0)
        hide_all(b3, 1)
        for n in range(4, count):
            ready(n)

        def give_in(b, r, j):
            sum_out(b, r, j)
            give(b, r, j, from_out, mid_give_in)

        def give_out(r, j):
            sum_in(b0, r, j)
            give(b0, r, j, from_in, mid_give_out)

        give_in(b2, 0, 0)
        own_branch()
        give_in(b2, 0, 1)

        @pl.loop(0, 2)
        def _(j):
            give_in(b2, 1, j)

        @pl.loop(2, PIECES)
        def _(j):
            for r in range(HALVES):
                give_in(b2, r, j)

        @pl.loop(0, PIECES)
        def _(j):
            give_in(b3, 0, j)

        @pl.loop(0, PIECES)
        def _(j):
            give_out(0, j)
            give_in(b3, 1, j)

        @pl.loop(0, PIECES)
        def _(j):
            give_out(1, j)

        for r in range(HALVES):

            @pl.loop(0, PIECES)
            def _(j):
                sum_in(own, r, j)
                sum_out(own, r, j)

            total = (
                branch[half(r)]
                + from_in[own, half(r)].astype(jnp.float32)
                + from_out[own, half(r)].astype(jnp.float32)
            )
            yield_out(half(r), total)

        for r in range(HALVES + 1):
            for b in (own, b0):
                mid_in(b, r).wait_send()
            for b in (own, b2, b3):
                mid_out(b, r).wait_send()

        @pl.loop(0, PIECES)
        def _(j):
            for r in range(HALVES):
                mid_give_in(b2, r, j).wait_send()
                mid_give_in(b3, r, j).wait_send()
                mid_give_out(b0, r, j).wait_send()

    @pl.when(sp < sp_size - 1)
    def _():
        edge_copy(0).wait_send()
        edge_copy(1).wait_send()

    proj_copy.wait_send()
    conv_copy(0).wait_send()
    conv_copy(1).wait_send()
    for j in range(PIECES):
        part_copy(j).wait_send()
    for n in range(count):
        x_hop(n).wait_send()
        near_hop(n, tp).wait_send()
        far_hop(n, tp).wait_send()
        relay_hop(n, far).wait_send()


def fused_layer(
    x_in, gate_b, gate_c, conv_taps, out_proj, mix_gain, resid, pre_gain, expert_gate, expert_up,
    expert_down, shared_gate, shared_up, shared_down, post_gain, routes, route_weights,
):
    experts = lax.axis_size("sp")
    line = experts // 2
    all_rows, channels = x_in.shape
    rows, width = resid.shape
    hid = expert_gate.shape[2]
    shared_hid = shared_gate.shape[1]
    dma = pltpu.SemaphoreType.DMA
    count = 2 * HALVES + PIECES
    bf, f32 = jnp.bfloat16, jnp.float32
    vmem = pl.BlockSpec(memory_space=pltpu.VMEM)
    hbm = pl.BlockSpec(memory_space=pltpu.HBM)
    lanes = 128 * (-(-experts // 128))
    pad = 16 * (-(-(conv_taps.shape[0] - 1) // 16))
    top = routes.shape[1]
    return pl.pallas_call(
        functools.partial(layer_kernel, line),
        out_shape=jax.ShapeDtypeStruct((rows, width), bf),
        in_specs=[hbm] * 17,
        out_specs=vmem,
        scratch_shapes=[
            pltpu.VMEM((all_rows, channels), bf),
            pltpu.VMEM((all_rows, channels), bf),
            pltpu.VMEM((all_rows, channels), bf),
            pltpu.VMEM(conv_taps.shape, bf),
            pltpu.VMEM((rows, width), bf),
            pltpu.VMEM((width,), bf),
            pltpu.VMEM((width,), bf),
            pltpu.VMEM((width,), bf),
            pltpu.VMEM((top, rows), jnp.int32),
            pltpu.VMEM((top, rows), f32),
            pltpu.VMEM((pad, channels), bf),
            pltpu.VMEM((pad, channels), bf),
            pltpu.VMEM((pad + all_rows, channels), f32),
            pltpu.VMEM((all_rows, channels), bf),
            pltpu.VMEM((2, rows, channels), bf),
            pltpu.VMEM((2, channels, width), bf),
            pltpu.VMEM((rows, width), bf),
            pltpu.VMEM((rows, width), bf),
            pltpu.VMEM((rows, width), f32),
            pltpu.VMEM((rows, width), bf),
            pltpu.VMEM((2, width, hid), bf),
            pltpu.VMEM((2, width, hid), bf),
            pltpu.VMEM((2 * hid, width), bf),
            pltpu.VMEM((width, shared_hid), bf),
            pltpu.VMEM((width, shared_hid), bf),
            pltpu.VMEM((shared_hid, width), bf),
            pltpu.VMEM((line, rows, width), bf),
            pltpu.VMEM((line, rows, lanes), f32),
            pltpu.VMEM((line, rows, 2 * hid), bf),
            pltpu.VMEM((rows, shared_hid), bf),
            pltpu.VMEM((rows, width), f32),
            pltpu.VMEM((line, rows, width), bf),
            pltpu.VMEM((line, rows, width), bf),
            pltpu.VMEM((line, rows, width), bf),
            dma((17,)),
            dma((2,)),
            dma((2,)),
            dma((1,)),
            dma((1,)),
            dma((2,)),
            dma((2,)),
            dma((PIECES,)),
            dma((PIECES,)),
        ]
        + [dma((count,))] * 8
        + [dma((line, HALVES + 1))] * 4
        + [dma((line, HALVES, PIECES))] * 4,
        compiler_params=pltpu.CompilerParams(
            collective_id=0, has_side_effects=True, vmem_limit_bytes=60 * 1024 * 1024
        ),
    )(
        x_in, gate_b, gate_c, conv_taps, resid, mix_gain, pre_gain, post_gain,
        routes.T, route_weights.T, out_proj, expert_gate, expert_up, expert_down,
        shared_gate, shared_up, shared_down,
    )


def passed_along(shard, axis, by):
    size = lax.axis_size(axis)
    pairs = [(i, i + by) for i in range(size) if 0 <= i + by < size]
    return lax.ppermute(shard, axis, pairs)


def body(
    x_in,
    gate_b,
    gate_c,
    conv_taps,
    out_proj,
    mix_gain,
    resid,
    pre_gain,
    expert_gate,
    expert_up,
    expert_down,
    shared_gate,
    shared_up,
    shared_down,
    post_gain,
    routes,
    route_weights,
):
    group = lax.axis_size("sp")
    wide_slots = 3 * resid.shape[0] * routes.shape[1] // group
    if wide_slots > resid.shape[0] and group == 2 * 2 * 2 and lax.axis_size("tp") == 2 * 2:
        return fused_layer(
            x_in, gate_b, gate_c, conv_taps, out_proj, mix_gain, resid, pre_gain, expert_gate,
            expert_up, expert_down, shared_gate, shared_up, shared_down, post_gain, routes,
            route_weights,
        )
    row_count = x_in.shape[0]
    channels = x_in.shape[1]
    reach = conv_taps.shape[0] - 1
    edge_rows = jnp.concatenate([x_in[row_count - reach :], gate_c[row_count - reach :]], 1)
    arrived_edge = passed_along(edge_rows, "sp", 1)
    inputs = jnp.concatenate([arrived_edge[:, :channels], x_in], 0).astype(jnp.float32)
    gate_rows = jnp.concatenate([arrived_edge[:, channels:], gate_c], 0).astype(jnp.float32)
    mixed_in = inputs * gate_rows
    taps = conv_taps.astype(jnp.float32)
    convolved = jnp.zeros((row_count, channels), jnp.float32)
    for index in range(reach + 1):
        convolved = convolved + taps[index][None, :] * mixed_in[index : index + row_count]
    conv_out = (gate_b.astype(jnp.float32) * convolved).astype(jnp.bfloat16)
    width_all = out_proj.shape[1]
    full_rows = lax.all_to_all(conv_out, "tp", split_axis=0, concat_axis=1, tiled=True)
    projected = jnp.dot(
        full_rows,
        lax.all_gather(out_proj, "tp", axis=0, tiled=True),
        preferred_element_type=jnp.float32,
    )
    row_scale = lax.rsqrt(jnp.mean(projected * projected, axis=1, keepdims=True) + epsilon)
    resid1 = (
        resid.astype(jnp.float32) + projected * row_scale * mix_gain.astype(jnp.float32)
    ).astype(jnp.bfloat16)
    wide_resid = resid1.astype(jnp.float32)
    normed = (
        wide_resid
        * lax.rsqrt(jnp.mean(wide_resid * wide_resid, axis=1, keepdims=True) + epsilon)
        * pre_gain.astype(jnp.float32)
    ).astype(jnp.bfloat16)
    experts = lax.axis_size("sp")
    local_rows = resid.shape[0]
    top_count = routes.shape[1]
    capacity = 3 * local_rows * top_count // (2 * experts)
    flat_ids = routes.reshape(-1)
    onehot = (flat_ids[:, None] == jnp.arange(experts, dtype=jnp.int32)[None, :]).astype(jnp.int32)
    before = jnp.cumsum(onehot, axis=0) - onehot
    position = jnp.sum(before * onehot, axis=1)
    slot_index = flat_ids * capacity + position
    outgoing = (
        jnp.zeros((experts * capacity, width_all), jnp.bfloat16)
        .at[slot_index]
        .set(jnp.repeat(normed, top_count, axis=0))
    )
    received = lax.all_to_all(
        outgoing.reshape(experts, capacity, width_all),
        "sp",
        split_axis=0,
        concat_axis=0,
        tiled=True,
    )
    arrived = received.reshape(experts * capacity, width_all)
    gate_h = jnp.dot(arrived, expert_gate[0], preferred_element_type=jnp.float32)
    up_h = jnp.dot(arrived, expert_up[0], preferred_element_type=jnp.float32)
    hidden = (jax.nn.silu(gate_h) * up_h).astype(jnp.bfloat16)
    expert_out = jnp.dot(hidden, expert_down[0], preferred_element_type=jnp.float32).astype(
        jnp.bfloat16
    )
    returned = lax.all_to_all(
        expert_out.reshape(experts, capacity, width_all),
        "sp",
        split_axis=0,
        concat_axis=0,
        tiled=True,
    )
    returned = returned.reshape(experts * capacity, width_all)
    picked = returned[slot_index].astype(jnp.float32).reshape(local_rows, top_count, width_all)
    routed = jnp.einsum("tk,tkd->td", route_weights, picked)
    shared_g = jnp.dot(normed, shared_gate, preferred_element_type=jnp.float32)
    shared_u = jnp.dot(normed, shared_up, preferred_element_type=jnp.float32)
    shared_hidden = (jax.nn.silu(shared_g) * shared_u).astype(jnp.bfloat16)
    shared_out = jnp.dot(shared_hidden, shared_down, preferred_element_type=jnp.float32)
    branch = routed + shared_out
    factor = lax.rsqrt(jnp.mean(branch * branch, axis=1, keepdims=True) + epsilon)
    return (wide_resid + branch * factor * post_gain.astype(jnp.float32)[None, :]).astype(
        jnp.bfloat16
    )


def solution(mesh):
    return jax.shard_map(
        body,
        mesh=mesh,
        in_specs=(
            P("sp", "tp"),
            P("sp", "tp"),
            P("sp", "tp"),
            P(None, "tp"),
            P("tp", None),
            P(),
            P(("sp", "tp"), None),
            P(),
            P("sp", None, None),
            P("sp", None, None),
            P("sp", None, None),
            P(),
            P(),
            P(),
            P(),
            P(("sp", "tp"), None),
            P(("sp", "tp"), None),
        ),
        out_specs=P(("sp", "tp"), None),
        check_vma=False,
    )
```

time: 103 us -> 131 us (1.27)
  the two profiles are of different devices: /device:TPU:0 before, /device:TPU:3 now
where the time goes in v2:
time: 131 us
  Pallas kernels  129 us (98%)
  local copies, waits for them, and re-layouts  1.88 us (1%)
    pallas_call x1, Pallas kernels, fused_layer(): pl.pallas_call(functools.partial(layer_kernel, line), out_shape=jax.Shape...  129 us

profile of v2, /device:TPU:3, one launch (start us, length us, event | category | flops | bytes accessed | tf_op | source)
XLA Modules:
  0.0 131.2 jit_solution(12074396595308108130)
XLA Ops:
  0.0 129.4 %shard_map.163 = bf16[128,2048]{1,0:T(8,128)(2,1)} custom-call(bf16[512,256]{1,0:T(8,128)(2,1)} %x_hbm.1, bf16[512,256]{1,0:T(8,128)(2,1)} %gate_b_hbm.1, bf16[512,256]{1,0:T(8,128)(2,1)} %gate_c_hbm.1, bf16[3,256]{1,0:T(4,128)(2,1)} %taps_hbm.1, bf16[128,2048]{1,0:T(8,128)(2,1)} %resid_hbm.1, bf16[2048]{0:T(1024)(128)(2,1)} %mix_hbm.1, ...), custom_call_target="tpu_custom_call" | custom-call | tf_op jit(solution)/shard_map/pallas_call | solution.py:751
  129.4 1.9 %copy.19 = bf16[128,2048]{1,0:T(8,128)(2,1)} copy(bf16[128,2048]{1,0:T(8,128)(2,1)} %shard_map.163) | data formatting | bytes 1048576

commit v3 on v2

--- a/solution.py
+++ b/solution.py
@@ -69,7 +69,9 @@
     outgoing,
     from_out,
     from_in,
+    out_v,
     load_sem,
+    out_sem,
     e_send,
     e_recv,
     p_send,
@@ -346,11 +348,6 @@
         met += jnp.where(jnp.where(x == 1, z < last, z > 0), 1, 0)
         pl.semaphore_wait(barrier, met)
 
-    for n in range(count):
-        x_hop(n).start()
-        if n in DIRECT:
-            direct_hop(n).start()
-
     loads[0].wait()
     loads[1].wait()
 
@@ -358,6 +355,11 @@
     def _():
         edge_copy(0).start()
         edge_copy(1).start()
+
+    for n in range(count):
+        x_hop(n).start()
+        if n - 1 in DIRECT or n == count - 1:
+            direct_hop(min(n, DIRECT[-1]) if n == count - 1 else n - 1).start()
 
     loads[2].wait()
     proj_copy.start()
@@ -510,12 +512,33 @@
                 shared_hidden[...], s_down[:, chunk(j)], preferred_element_type=jnp.float32
             )
 
-    def yield_out(part, total):
+    def out_copy(r):
+        return pltpu.make_async_copy(out_v.at[half(r)], out_ref.at[half(r)], out_sem.at[r])
+
+    def yield_out(r, total):
         factor = lax.rsqrt(jnp.mean(total * total, axis=1, keepdims=True) + epsilon)
-        out_ref[part] = (
-            resid1[part].astype(jnp.float32)
+        out_v[half(r)] = (
+            resid1[half(r)].astype(jnp.float32)
             + total * factor * post_ref[...].astype(jnp.float32).reshape(1, width)
         ).astype(jnp.bfloat16)
+        out_copy(r).start()
+
+    def settle():
+        @pl.when(sp < sp_size - 1)
+        def _():
+            edge_copy(0).wait_send()
+            edge_copy(1).wait_send()
+
+        proj_copy.wait_send()
+        conv_copy(0).wait_send()
+        conv_copy(1).wait_send()
+        for j in range(PIECES):
+            part_copy(j).wait_send()
+        for n in range(count):
+            x_hop(n).wait_send()
+            near_hop(n, tp).wait_send()
+            far_hop(n, tp).wait_send()
+            relay_hop(n, far).wait_send()
 
     for load in loads[10:14]:
         load.wait()
@@ -523,6 +546,7 @@
     shared_up_to_hidden()
     relay(0)
     spread(3)
+    spread(4)
     for load in loads[14:]:
         load.wait()
 
@@ -533,32 +557,29 @@
         got_in(b1, 0)
         hide(b1, 0, half_rows, 0)
         relay(1)
-        relay(3)
         got_in(b1, 1)
         hide(b1, half_rows, half_rows, 0)
-        spread(4)
+        relay(3)
         relay(2)
         spread(5)
-        got_in(b2, TABLE)
-        got_in(b3, TABLE)
         for n in range(4):
             ready(n)
         hide_all(b1, 1)
-        hide_all(own, 1)
         relay(4)
         spread(6)
-        got_in(b2, 0)
-        hide_half(b2, 0)
         ready(4)
         for r in range(HALVES):
             give(b1, r, 0, None, edge_give)
+        got_in(b2, TABLE)
+        got_in(b2, 0)
+        hide_half(b2, 0)
         give(b2, 0, 0, None, edge_give)
         relay(5)
         spread(7)
         ready(5)
-        give(b2, 0, 1, None, edge_give)
         for r in range(HALVES):
             give(b1, r, 1, None, edge_give)
+        give(b2, 0, 1, None, edge_give)
         relay(6)
         relay(7)
         got_in(b2, 1)
@@ -573,10 +594,10 @@
 
         @pl.loop(2, PIECES)
         def _(j):
-            for r in range(HALVES):
-                give(b2, r, j, None, edge_give)
-
-        own_branch()
+            give(b2, 0, j, None, edge_give)
+
+        hide_all(own, 1)
+        got_in(b3, TABLE)
         for r in range(HALVES):
             got_in(b3, r)
             hide_half(b3, r)
@@ -587,8 +608,23 @@
 
         @pl.loop(2, PIECES)
         def _(j):
+            give(b2, 1, j, None, edge_give)
+
+        @pl.loop(2, PIECES)
+        def _(j):
             for r in range(HALVES):
                 give(b1, r, j, None, edge_give)
+
+        own_branch()
+        settle()
+        for r in range(HALVES + 1):
+            edge_in(own, r).wait_send()
+
+        @pl.loop(0, PIECES)
+        def _(j):
+            for b in (b2, b3):
+                for r in range(HALVES):
+                    edge_give(b, r, j).wait_send()
 
         for r in range(HALVES):
 
@@ -597,16 +633,12 @@
                 sum_in(own, r, j)
 
             total = branch[half(r)] + from_in[own, half(r)].astype(jnp.float32)
-            yield_out(half(r), total)
-
-        for r in range(HALVES + 1):
-            edge_in(own, r).wait_send()
+            yield_out(r, total)
 
         @pl.loop(0, PIECES)
         def _(j):
-            for b in (b1, b2, b3):
-                for r in range(HALVES):
-                    edge_give(b, r, j).wait_send()
+            for r in range(HALVES):
+                edge_give(b1, r, j).wait_send()
 
     @pl.when(level == 1)
     def _():
@@ -626,29 +658,28 @@
         pass_out(b2, 0)
         pass_out(b3, TABLE)
         relay(1)
-        relay(3)
         pass_in(1)
         pass_out(b2, 1)
+        relay(3)
         hide_all(b0, 0)
-        spread(4)
-        hide_all(b2, 0)
         relay(2)
         spread(5)
+        hide_all(b2, 0)
         for n in range(4):
             ready(n)
-        hide_all(b2, 1)
         relay(4)
         spread(6)
-        hide_all(own, 1)
+        hide_all(b2, 1)
         pass_out(b3, 0)
         relay(5)
         spread(7)
-        hide_all(b0, 1)
+        hide_all(own, 1)
         relay(6)
         relay(7)
         pass_out(b3, 1)
         hide_all(b3, 0)
         hide_all(b3, 1)
+        hide_all(b0, 1)
         for n in range(4, count):
             ready(n)
 
@@ -661,8 +692,8 @@
             give(b0, r, j, from_in, mid_give_out)
 
         give_in(b2, 0, 0)
+        give_in(b2, 0, 1)
         own_branch()
-        give_in(b2, 0, 1)
 
         @pl.loop(0, 2)
         def _(j):
@@ -670,21 +701,38 @@
 
         @pl.loop(2, PIECES)
         def _(j):
-            for r in range(HALVES):
-                give_in(b2, r, j)
+            give_in(b2, 0, j)
 
         @pl.loop(0, PIECES)
         def _(j):
             give_in(b3, 0, j)
+
+        settle()
 
         @pl.loop(0, PIECES)
         def _(j):
             give_out(0, j)
             give_in(b3, 1, j)
 
+        give_out(1, 0)
+        give_out(1, 1)
+
+        @pl.loop(2, PIECES)
+        def _(j):
+            give_in(b2, 1, j)
+            give_out(1, j)
+
+        for r in range(HALVES + 1):
+            for b in (own, b0):
+                mid_in(b, r).wait_send()
+            for b in (own, b2, b3):
+                mid_out(b, r).wait_send()
+
         @pl.loop(0, PIECES)
         def _(j):
-            give_out(1, j)
+            mid_give_in(b2, 0, j).wait_send()
+            mid_give_in(b3, 0, j).wait_send()
+            mid_give_in(b3, 1, j).wait_send()
 
         for r in range(HALVES):
 
@@ -698,36 +746,16 @@
                 + from_in[own, half(r)].astype(jnp.float32)
                 + from_out[own, half(r)].astype(jnp.float32)
             )
-            yield_out(half(r), total)
-
-        for r in range(HALVES + 1):
-            for b in (own, b0):
-                mid_in(b, r).wait_send()
-            for b in (own, b2, b3):
-                mid_out(b, r).wait_send()
+            yield_out(r, total)
 
         @pl.loop(0, PIECES)
         def _(j):
+            mid_give_in(b2, 1, j).wait_send()
             for r in range(HALVES):
-                mid_give_in(b2, r, j).wait_send()
-                mid_give_in(b3, r, j).wait_send()
                 mid_give_out(b0, r, j).wait_send()
 
-    @pl.when(sp < sp_size - 1)
-    def _():
-        edge_copy(0).wait_send()
-        edge_copy(1).wait_send()
-
-    proj_copy.wait_send()
-    conv_copy(0).wait_send()
-    conv_copy(1).wait_send()
-    for j in range(PIECES):
-        part_copy(j).wait_send()
-    for n in range(count):
-        x_hop(n).wait_send()
-        near_hop(n, tp).wait_send()
-        far_hop(n, tp).wait_send()
-        relay_hop(n, far).wait_send()
+    for r in range(HALVES):
+        out_copy(r).wait()
 
 
 def fused_layer(
@@ -743,7 +771,6 @@
     dma = pltpu.SemaphoreType.DMA
     count = 2 * HALVES + PIECES
     bf, f32 = jnp.bfloat16, jnp.float32
-    vmem = pl.BlockSpec(memory_space=pltpu.VMEM)
     hbm = pl.BlockSpec(memory_space=pltpu.HBM)
     lanes = 128 * (-(-experts // 128))
     pad = 16 * (-(-(conv_taps.shape[0] - 1) // 16))
@@ -752,7 +779,7 @@
         functools.partial(layer_kernel, line),
         out_shape=jax.ShapeDtypeStruct((rows, width), bf),
         in_specs=[hbm] * 17,
-        out_specs=vmem,
+        out_specs=hbm,
         scratch_shapes=[
             pltpu.VMEM((all_rows, channels), bf),
             pltpu.VMEM((all_rows, channels), bf),
@@ -788,7 +815,9 @@
             pltpu.VMEM((line, rows, width), bf),
             pltpu.VMEM((line, rows, width), bf),
             pltpu.VMEM((line, rows, width), bf),
+            pltpu.VMEM((rows, width), bf),
             dma((17,)),
+            dma((HALVES,)),
             dma((2,)),
             dma((2,)),
             dma((1,)),

time: 131 us -> 85.1 us (0.65)
  the two profiles are of different devices: /device:TPU:3 before, /device:TPU:0 now
where the time goes in v3:
time: 85.1 us; the launch traced here: 85 us
  Pallas kernels  83.1 us (98%)
  local copies, waits for them, and re-layouts  1.88 us (2%)
    pallas_call x1, Pallas kernels, fused_layer(): pl.pallas_call(functools.partial(layer_kernel, line), out_shape=jax.Shape...  83.1 us
    unnamed x1, local copies, waits for them, and re-layouts  1.88 us

profile of v3, /device:TPU:0, one launch (start us, length us, event | category | flops | bytes accessed | tf_op | source)
XLA Modules:
  0.0 85.0 jit_solution(16225072519664534440)
XLA Ops:
  0.0 83.1 %shard_map.163 = bf16[128,2048]{1,0:T(8,128)(2,1)} custom-call(bf16[512,256]{1,0:T(8,128)(2,1)} %x_hbm.1, bf16[512,256]{1,0:T(8,128)(2,1)} %gate_b_hbm.1, bf16[512,256]{1,0:T(8,128)(2,1)} %gate_c_hbm.1, bf16[3,256]{1,0:T(4,128)(2,1)} %taps_hbm.1, bf16[128,2048]{1,0:T(8,128)(2,1)} %resid_hbm.1, bf16[2048]{0:T(1024)(128)(2,1)} %mix_hbm.1, ...), custom_call_target="tpu_custom_call" | custom-call | tf_op jit(solution)/shard_map/pallas_call | solution.py:778
  83.1 1.9 %copy.19 = bf16[128,2048]{1,0:T(8,128)(2,1)} copy(bf16[128,2048]{1,0:T(8,128)(2,1)} %shard_map.163) | data formatting | bytes 1048576

commit v4 on v3

--- a/solution.py
+++ b/solution.py
@@ -12,6 +12,7 @@
 PIECES = 4
 HALVES = 2
 DIRECT = (3, 7)
+ORDER = (0, 1, 2, 3, 4, -3, 5, 6, 7, -7)
 TABLE = HALVES
 
 
@@ -72,28 +73,22 @@
     out_v,
     load_sem,
     out_sem,
-    e_send,
+    edge_send,
+    misc_send,
+    spread_send,
+    relay_send,
+    in_send,
+    out_send,
     e_recv,
-    p_send,
     p_recv,
-    c_send,
     c_recv,
-    f_send,
     f_recv,
-    wx_send,
     wx_recv,
-    wn_send,
     wn_recv,
-    wf_send,
     wf_recv,
-    wr_send,
     wr_recv,
-    gi_send,
-    go_send,
     gi_recv,
     go_recv,
-    ri_send,
-    ro_send,
     ri_recv,
     ro_recv,
 ):
@@ -176,34 +171,26 @@
     pad = edge_x.shape[0]
 
     def edge_copy(n):
-        source, landing = ((x_ref, edge_x), (gate_c_ref, edge_c))[n]
+        source, landing = ((x_hbm, edge_x), (gate_c_hbm, edge_c))[n]
         return pltpu.make_async_remote_copy(
             src_ref=source.at[pl.ds(all_rows - pad, pad)],
             dst_ref=landing,
-            send_sem=e_send.at[n],
+            send_sem=edge_send.at[0],
             recv_sem=e_recv.at[n],
             device_id=((sp + 1) % sp_size, tp),
             device_id_type=MESH,
         )
 
-    proj_copy = pltpu.make_async_remote_copy(
-        src_ref=proj.at[0],
-        dst_ref=proj.at[1],
-        send_sem=p_send.at[0],
-        recv_sem=p_recv.at[0],
-        device_id=(sp, near),
-        device_id_type=MESH,
-    )
-
     def block_rows(owner):
         return pl.ds(pl.multiple_of(owner * rows, rows), rows)
 
-    def conv_copy(n):
+    def conv_copy(n, k):
+        begin, size = ((pad, rows - pad), (0, pad))[k]
         return pltpu.make_async_remote_copy(
-            src_ref=conv.at[block_rows((near, near_far)[n])],
-            dst_ref=conv_near.at[n],
-            send_sem=c_send.at[n],
-            recv_sem=c_recv.at[n],
+            src_ref=conv.at[pl.ds(pl.multiple_of((near, near_far)[n] * rows + begin, pad), size)],
+            dst_ref=conv_near.at[n, pl.ds(begin, size)],
+            send_sem=misc_send.at[0],
+            recv_sem=c_recv.at[n, k],
             device_id=(sp, near),
             device_id_type=MESH,
         )
@@ -214,15 +201,35 @@
     def half(r):
         return pl.ds(r * half_rows, half_rows)
 
+    def proj_copy(j):
+        return pltpu.make_async_remote_copy(
+            src_ref=proj.at[0, :, chunk(j)],
+            dst_ref=proj.at[1, :, chunk(j)],
+            send_sem=misc_send.at[0],
+            recv_sem=p_recv.at[j],
+            device_id=(sp, near),
+            device_id_type=MESH,
+        )
+
     def part_copy(j):
+        where = (pl.ds(pad, rows - pad), chunk(j))
         return pltpu.make_async_remote_copy(
-            src_ref=part_out.at[:, chunk(j)],
-            dst_ref=part_in.at[:, chunk(j)],
-            send_sem=f_send.at[j],
+            src_ref=part_out.at[where],
+            dst_ref=part_in.at[where],
+            send_sem=misc_send.at[0],
             recv_sem=f_recv.at[j],
             device_id=(sp, far),
             device_id_type=MESH,
         )
+
+    part_head = pltpu.make_async_remote_copy(
+        src_ref=part_out.at[pl.ds(0, pad)],
+        dst_ref=part_in.at[pl.ds(0, pad)],
+        send_sem=misc_send.at[0],
+        recv_sem=f_recv.at[PIECES],
+        device_id=(sp, far),
+        device_id_type=MESH,
+    )
 
     pieces = []
     for ref, held in ((eg_ref, w_gate), (eu_ref, w_up)):
@@ -250,26 +257,40 @@
         return pltpu.make_async_remote_copy(
             src_ref=source if first else landing,
             dst_ref=landing,
-            send_sem=send.at[n],
-            recv_sem=recv.at[n],
+            send_sem=send.at[0],
+            recv_sem=recv,
             device_id=target,
             device_id_type=MESH,
         )
 
+    def late(n):
+        return max(0, n - 2 * HALVES + 1)
+
     def x_hop(n):
-        return hop(n, tp, (mate, tp), wx_send, wx_recv, True)
+        return hop(n, tp, (mate, tp), spread_send, wx_recv.at[n], True)
 
     def near_hop(n, owner):
-        return hop(n, owner, (sp, near), wn_send, wn_recv)
+        return hop(n, owner, (sp, near), spread_send, wn_recv.at[late(n)])
 
     def far_hop(n, owner):
-        return hop(n, owner, (sp, far), wf_send, wf_recv)
+        return hop(n, owner, (sp, far), relay_send, wf_recv.at[n])
 
     def direct_hop(n):
-        return hop(n, far, (mate, tp), wf_send, wf_recv, True)
+        return hop(n, far, (mate, tp), relay_send, wf_recv.at[n], True)
 
     def relay_hop(n, owner):
-        return hop(n, owner, (sp, near), wr_send, wr_recv)
+        return hop(n, owner, (sp, near), relay_send, wr_recv.at[late(n)])
+
+    def drain(send, recv, size):
+        where = w_down.at[pl.ds(0, size)]
+        return pltpu.make_async_remote_copy(
+            src_ref=where,
+            dst_ref=where,
+            send_sem=send.at[0],
+            recv_sem=recv.at[0],
+            device_id=(sp, near),
+            device_id_type=MESH,
+        )
 
     def spread(n):
         with jax.named_scope("w_x"):
@@ -288,119 +309,102 @@
             near_hop(n, near).wait_recv()
             relay_hop(n, near_far).wait_recv()
 
+    def ready_both():
+        size = 2 * hid // tp_size
+        with jax.named_scope("w_ready"):
+            drain(spread_send, wn_recv, size).wait_recv()
+            drain(relay_send, wr_recv, size).wait_recv()
+
     def block_copy(b, r, target, send, recv):
         ref = shares.at[b] if r == TABLE else blocks.at[b, half(r)]
         return pltpu.make_async_remote_copy(
             src_ref=ref,
             dst_ref=ref,
-            send_sem=send.at[b, r],
-            recv_sem=recv.at[b, r],
+            send_sem=send.at[0],
+            recv_sem=recv,
             device_id=target,
             device_id_type=MESH,
         )
 
-    def edge_in(b, r):
-        return block_copy(b, r, inward, gi_send, go_recv)
-
-    def mid_in(b, r):
-        return block_copy(b, r, inward, gi_send, gi_recv)
-
-    def mid_out(b, r):
-        return block_copy(b, r, outward, go_send, gi_recv)
-
-    def got_in(b, r):
+    def edge_in(r):
+        return block_copy(rel(0), r, inward, in_send, go_recv.at[r])
+
+    def mid_in(k, r):
+        return block_copy(rel(k), r, inward, in_send, gi_recv.at[last - k - 1, r])
+
+    def mid_out(k, r):
+        return block_copy(rel(k), r, outward, out_send, gi_recv.at[k - 1, r])
+
+    def got_in(k, r):
         with jax.named_scope("w_gi"):
-            block_copy(b, r, inward, gi_send, gi_recv).wait_recv()
-
-    def got_out(b, r):
+            block_copy(rel(k), r, inward, in_send, gi_recv.at[k - 1, r]).wait_recv()
+
+    def got_out(r):
         with jax.named_scope("w_go"):
-            block_copy(b, r, outward, go_send, go_recv).wait_recv()
-
-    def sum_copy(b, r, j, landing, target, send, recv):
+            block_copy(rel(0), r, outward, out_send, go_recv.at[r]).wait_recv()
+
+    def sum_copy(k, r, j, landing, target, send, recv):
         return pltpu.make_async_remote_copy(
-            src_ref=outgoing.at[b, half(r), chunk(j)],
-            dst_ref=landing.at[b, half(r), chunk(j)],
-            send_sem=send.at[b, r, j],
-            recv_sem=recv.at[b, r, j],
+            src_ref=outgoing.at[rel(k), half(r), chunk(j)],
+            dst_ref=landing.at[rel(k), half(r), chunk(j)],
+            send_sem=send.at[0],
+            recv_sem=recv.at[j],
             device_id=target,
             device_id_type=MESH,
         )
 
-    def edge_give(b, r, j):
-        return sum_copy(b, r, j, from_out, inward, ri_send, ro_recv)
-
-    def mid_give_in(b, r, j):
-        return sum_copy(b, r, j, from_in, inward, ri_send, ri_recv)
-
-    def mid_give_out(b, r, j):
-        return sum_copy(b, r, j, from_in, outward, ro_send, ri_recv)
-
-    def sum_in(b, r, j):
+    def edge_give(k, r, j):
+        return sum_copy(k, r, j, from_out, inward, in_send, ro_recv.at[k - 1, r])
+
+    def mid_give_in(k, r, j):
+        return sum_copy(k, r, j, from_in, inward, in_send, ri_recv.at[last - k, r])
+
+    def mid_give_out(k, r, j):
+        return sum_copy(k, r, j, from_in, outward, out_send, ri_recv.at[k, r])
+
+    def sum_in(k, r, j):
         with jax.named_scope("w_ri"):
-            sum_copy(b, r, j, from_in, inward, ri_send, ri_recv).wait_recv()
-
-    def sum_out(b, r, j):
+            sum_copy(k, r, j, from_in, inward, in_send, ri_recv.at[k, r]).wait_recv()
+
+    def sum_out(k, r, j):
         with jax.named_scope("w_ro"):
-            sum_copy(b, r, j, from_out, outward, ro_send, ro_recv).wait_recv()
+            sum_copy(k, r, j, from_out, outward, out_send, ro_recv.at[k - 1, r]).wait_recv()
 
     with jax.named_scope("w_barrier"):
         met = 3 + jnp.where(z > 0, 1, 0) + jnp.where(z < last, 1, 0)
         met += jnp.where(jnp.where(x == 1, z < last, z > 0), 1, 0)
         pl.semaphore_wait(barrier, met)
 
-    loads[0].wait()
-    loads[1].wait()
-
     @pl.when(sp < sp_size - 1)
     def _():
         edge_copy(0).start()
         edge_copy(1).start()
 
-    for n in range(count):
-        x_hop(n).start()
-        if n - 1 in DIRECT or n == count - 1:
-            direct_hop(min(n, DIRECT[-1]) if n == count - 1 else n - 1).start()
+    for n in ORDER:
+        if n < 0:
+            direct_hop(-n).start()
+        else:
+            x_hop(n).start()
 
     loads[2].wait()
-    proj_copy.start()
+    for j in range(PIECES):
+        proj_copy(j).start()
+
+    for n in (0, 1, 3, 4):
+        loads[n].wait()
+    mixed[:pad] = jnp.zeros((pad, channels), jnp.float32)
     mixed[pad:] = x_ref[...].astype(jnp.float32) * gate_c_ref[...].astype(jnp.float32)
-    loads[3].wait()
-    loads[4].wait()
-
-    with jax.named_scope("w_edge"):
-
-        @pl.when(sp > 0)
-        def _():
-            edge_copy(0).wait_recv()
-            edge_copy(1).wait_recv()
-            mixed[:pad] = edge_x[...].astype(jnp.float32) * edge_c[...].astype(jnp.float32)
-
-        @pl.when(sp == 0)
-        def _():
-            mixed[:pad] = jnp.zeros((pad, channels), jnp.float32)
-
-    convolved = jnp.zeros((all_rows, channels), jnp.float32)
-    for k in range(reach + 1):
-        begin = pad - reach + k
-        convolved += taps_ref[k : k + 1].astype(jnp.float32) * mixed[begin : begin + all_rows]
-    conv[...] = (gate_b_ref[...].astype(jnp.float32) * convolved).astype(jnp.bfloat16)
-    conv_copy(1).start()
-    conv_copy(0).start()
-
-    def project(n, owner, cols):
-        return jnp.dot(
-            conv[block_rows(owner)], proj[0, :, cols], preferred_element_type=jnp.float32
-        ) + jnp.dot(conv_near[n], proj[1, :, cols], preferred_element_type=jnp.float32)
-
-    with jax.named_scope("w_conv"):
-        proj_copy.wait_recv()
-        conv_copy(1).wait_recv()
-
-    @pl.loop(0, PIECES)
-    def _(j):
-        part_out[:, chunk(j)] = project(1, far, chunk(j)).astype(jnp.bfloat16)
-        part_copy(j).start()
-
+
+    def convolve(size):
+        convolved = jnp.zeros((size, channels), jnp.float32)
+        for k in range(reach + 1):
+            begin = pad - reach + k
+            convolved += taps_ref[k : k + 1].astype(jnp.float32) * mixed[begin : begin + size]
+        conv[:size] = (gate_b_ref[:size].astype(jnp.float32) * convolved).astype(jnp.bfloat16)
+
+    convolve(all_rows)
+    conv_copy(1, 0).start()
+    conv_copy(0, 0).start()
     loads[5].wait()
     loads[6].wait()
     lanes = lax.broadcasted_iota(jnp.int32, (rows, shares.shape[2]), 1)
@@ -408,24 +412,63 @@
     table = jnp.zeros((shares.shape[2], rows), jnp.float32)
     for k in range(routes_ref.shape[0]):
         table += jnp.where(names == routes_ref[k : k + 1], weights_ref[k : k + 1], 0.0)
-    shares[z] = table.T
-
     own = z
-
-    @pl.when(level == 0)
-    def _():
-        edge_in(own, TABLE).start()
-
-    @pl.when(level == 1)
-    def _():
-        mid_in(own, TABLE).start()
-        mid_out(own, TABLE).start()
-
-    conv_copy(0).wait_recv()
+    shares[own] = table.T
+
+    def send_own(r):
+        @pl.when(level == 0)
+        def _():
+            edge_in(r).start()
+
+        @pl.when(level == 1)
+        def _():
+            mid_in(1, r).start()
+            mid_out(1, r).start()
+
+    send_own(TABLE)
+
+    def project(n, owner, cols, begin, size):
+        mine = pl.ds(pl.multiple_of(owner * rows + begin, pad), size)
+        return jnp.dot(
+            conv[mine], proj[0, :, cols], preferred_element_type=jnp.float32
+        ) + jnp.dot(
+            conv_near[n, begin : begin + size], proj[1, :, cols], preferred_element_type=jnp.float32
+        )
+
+    with jax.named_scope("w_conv"):
+        conv_copy(1, 0).wait_recv()
 
     @pl.loop(0, PIECES)
     def _(j):
-        projected[:, chunk(j)] = project(0, tp, chunk(j))
+        proj_copy(j).wait_recv()
+        part_out[pad:, chunk(j)] = project(1, far, chunk(j), pad, rows - pad).astype(jnp.bfloat16)
+        part_copy(j).start()
+
+    with jax.named_scope("w_edge"):
+
+        @pl.when(sp > 0)
+        def _():
+            edge_copy(0).wait_recv()
+            edge_copy(1).wait_recv()
+            mixed[:pad] = edge_x[...].astype(jnp.float32) * edge_c[...].astype(jnp.float32)
+
+    convolve(pad)
+    conv_copy(1, 1).start()
+    conv_copy(0, 1).start()
+    with jax.named_scope("w_head"):
+        conv_copy(1, 1).wait_recv()
+
+    @pl.loop(0, PIECES)
+    def _(j):
+        part_out[:pad, chunk(j)] = project(1, far, chunk(j), 0, pad).astype(jnp.bfloat16)
+
+    part_head.start()
+    conv_copy(0, 0).wait_recv()
+    conv_copy(0, 1).wait_recv()
+
+    @pl.loop(0, PIECES)
+    def _(j):
+        projected[:, chunk(j)] = project(0, tp, chunk(j), 0, rows)
 
     spread(0)
     spread(1)
@@ -437,7 +480,10 @@
         @pl.loop(0, PIECES)
         def _(j):
             part_copy(j).wait_recv()
-            projected[:, chunk(j)] += part_in[:, chunk(j)].astype(jnp.float32)
+            projected[pad:, chunk(j)] += part_in[pad:, chunk(j)].astype(jnp.float32)
+
+        part_head.wait_recv()
+        projected[:pad] += part_in[:pad].astype(jnp.float32)
 
     with jax.named_scope("norm"):
         for r in range(HALVES):
@@ -455,14 +501,7 @@
                 wide * normal * pre_ref[...].astype(jnp.float32).reshape(1, width)
             ).astype(jnp.bfloat16)
 
-            @pl.when(level == 0)
-            def _():
-                edge_in(own, r).start()
-
-            @pl.when(level == 1)
-            def _():
-                mid_in(own, r).start()
-                mid_out(own, r).start()
+            send_own(r)
 
     spread(2)
 
@@ -493,12 +532,12 @@
             hidden[b, part], w_down[:, chunk(j)], preferred_element_type=jnp.float32
         )
 
-    def give(b, r, j, arrived, send):
-        made = down(b, half(r), j)
+    def give(k, r, j, arrived, send):
+        made = down(rel(k), half(r), j)
         if arrived is not None:
-            made += arrived[b, half(r), chunk(j)].astype(jnp.float32)
-        outgoing[b, half(r), chunk(j)] = made.astype(jnp.bfloat16)
-        send(b, r, j).start()
+            made += arrived[rel(k), half(r), chunk(j)].astype(jnp.float32)
+        outgoing[rel(k), half(r), chunk(j)] = made.astype(jnp.bfloat16)
+        send(k, r, j).start()
 
     def shared_up_to_hidden():
         s_g = jnp.dot(blocks[own], s_gate[...], preferred_element_type=jnp.float32)
@@ -526,19 +565,14 @@
     def settle():
         @pl.when(sp < sp_size - 1)
         def _():
-            edge_copy(0).wait_send()
-            edge_copy(1).wait_send()
-
-        proj_copy.wait_send()
-        conv_copy(0).wait_send()
-        conv_copy(1).wait_send()
-        for j in range(PIECES):
-            part_copy(j).wait_send()
-        for n in range(count):
-            x_hop(n).wait_send()
-            near_hop(n, tp).wait_send()
-            far_hop(n, tp).wait_send()
-            relay_hop(n, far).wait_send()
+            drain(edge_send, e_recv, 2 * pad * channels // width).wait_send()
+
+        drain(misc_send, e_recv, channels + 2 * rows * channels // width + rows).wait_send()
+        drain(spread_send, e_recv, 2 * 3 * hid // tp_size).wait_send()
+        drain(relay_send, e_recv, 2 * 3 * hid // tp_size).wait_send()
+
+    sent_block = rows + 2 * rows * shares.shape[2] // width
+    sent_sums = rows
 
     for load in loads[10:14]:
         load.wait()
@@ -546,200 +580,175 @@
     shared_up_to_hidden()
     relay(0)
     spread(3)
-    spread(4)
     for load in loads[14:]:
         load.wait()
 
     @pl.when(level == 0)
     def _():
-        b1, b2, b3 = rel(1), rel(2), rel(3)
-        got_in(b1, TABLE)
-        got_in(b1, 0)
-        hide(b1, 0, half_rows, 0)
+        got_in(1, TABLE)
+        got_in(1, 0)
+        hide(rel(1), 0, half_rows, 0)
+        spread(4)
         relay(1)
-        got_in(b1, 1)
-        hide(b1, half_rows, half_rows, 0)
+        got_in(1, 1)
+        hide(rel(1), half_rows, half_rows, 0)
+        relay(2)
         relay(3)
-        relay(2)
+        ready_both()
+        hide_all(rel(1), 1)
+        relay(4)
         spread(5)
-        for n in range(4):
-            ready(n)
-        hide_all(b1, 1)
-        relay(4)
-        spread(6)
         ready(4)
         for r in range(HALVES):
-            give(b1, r, 0, None, edge_give)
-        got_in(b2, TABLE)
-        got_in(b2, 0)
-        hide_half(b2, 0)
-        give(b2, 0, 0, None, edge_give)
+            give(1, r, 0, None, edge_give)
+        spread(6)
+        got_in(2, TABLE)
+        got_in(2, 0)
+        hide_half(rel(2), 0)
+        give(2, 0, 0, None, edge_give)
         relay(5)
         spread(7)
         ready(5)
         for r in range(HALVES):
-            give(b1, r, 1, None, edge_give)
-        give(b2, 0, 1, None, edge_give)
+            give(1, r, 1, None, edge_give)
+        give(2, 0, 1, None, edge_give)
         relay(6)
         relay(7)
-        got_in(b2, 1)
-        hide_half(b2, 1)
+        got_in(2, 1)
+        hide_half(rel(2), 1)
 
         @pl.loop(0, 2)
         def _(j):
-            give(b2, 1, j, None, edge_give)
+            give(2, 1, j, None, edge_give)
 
         ready(6)
         ready(7)
 
         @pl.loop(2, PIECES)
         def _(j):
-            give(b2, 0, j, None, edge_give)
+            give(2, 0, j, None, edge_give)
 
         hide_all(own, 1)
-        got_in(b3, TABLE)
+        got_in(3, TABLE)
         for r in range(HALVES):
-            got_in(b3, r)
-            hide_half(b3, r)
+            got_in(3, r)
+            hide_half(rel(3), r)
 
             @pl.loop(0, PIECES)
             def _(j):
-                give(b3, r, j, None, edge_give)
+                give(3, r, j, None, edge_give)
 
         @pl.loop(2, PIECES)
         def _(j):
-            give(b2, 1, j, None, edge_give)
+            give(2, 1, j, None, edge_give)
 
         @pl.loop(2, PIECES)
         def _(j):
             for r in range(HALVES):
-                give(b1, r, j, None, edge_give)
+                give(1, r, j, None, edge_give)
 
         own_branch()
         settle()
-        for r in range(HALVES + 1):
-            edge_in(own, r).wait_send()
-
-        @pl.loop(0, PIECES)
-        def _(j):
-            for b in (b2, b3):
-                for r in range(HALVES):
-                    edge_give(b, r, j).wait_send()
-
         for r in range(HALVES):
 
             @pl.loop(0, PIECES)
             def _(j):
-                sum_in(own, r, j)
+                sum_in(0, r, j)
 
             total = branch[half(r)] + from_in[own, half(r)].astype(jnp.float32)
             yield_out(r, total)
 
-        @pl.loop(0, PIECES)
-        def _(j):
-            for r in range(HALVES):
-                edge_give(b1, r, j).wait_send()
+        drain(in_send, e_recv, sent_block + 3 * sent_sums).wait_send()
 
     @pl.when(level == 1)
     def _():
-        b0, b2, b3 = rel(0), rel(2), rel(3)
-
         def pass_in(r):
-            got_out(b0, r)
-            mid_in(b0, r).start()
-
-        def pass_out(b, r):
-            got_in(b, r)
-            mid_out(b, r).start()
+            got_out(r)
+            mid_in(0, r).start()
+
+        def pass_out(k, r):
+            got_in(k, r)
+            mid_out(k, r).start()
 
         pass_in(TABLE)
-        pass_out(b2, TABLE)
+        pass_out(2, TABLE)
         pass_in(0)
-        pass_out(b2, 0)
-        pass_out(b3, TABLE)
+        pass_out(2, 0)
+        pass_out(3, TABLE)
+        spread(4)
         relay(1)
         pass_in(1)
-        pass_out(b2, 1)
+        pass_out(2, 1)
+        hide_all(rel(0), 0)
+        relay(2)
         relay(3)
-        hide_all(b0, 0)
-        relay(2)
+        hide_all(rel(2), 0)
+        relay(4)
         spread(5)
-        hide_all(b2, 0)
-        for n in range(4):
-            ready(n)
-        relay(4)
+        ready_both()
+        pass_out(3, 0)
+        hide_all(rel(2), 1)
         spread(6)
-        hide_all(b2, 1)
-        pass_out(b3, 0)
         relay(5)
         spread(7)
         hide_all(own, 1)
+        pass_out(3, 1)
         relay(6)
         relay(7)
-        pass_out(b3, 1)
-        hide_all(b3, 0)
-        hide_all(b3, 1)
-        hide_all(b0, 1)
+        hide_all(rel(3), 0)
+        hide_all(rel(3), 1)
+        hide_all(rel(0), 1)
         for n in range(4, count):
             ready(n)
 
-        def give_in(b, r, j):
-            sum_out(b, r, j)
-            give(b, r, j, from_out, mid_give_in)
+        def give_in(k, r, j):
+            sum_out(k, r, j)
+            give(k, r, j, from_out, mid_give_in)
 
         def give_out(r, j):
-            sum_in(b0, r, j)
-            give(b0, r, j, from_in, mid_give_out)
-
-        give_in(b2, 0, 0)
-        give_in(b2, 0, 1)
+            sum_in(0, r, j)
+            give(0, r, j, from_in, mid_give_out)
+
+        @pl.loop(0, 2)
+        def _(j):
+            give_in(2, 0, j)
+
         own_branch()
 
         @pl.loop(0, 2)
         def _(j):
-            give_in(b2, 1, j)
+            give_in(2, 1, j)
 
         @pl.loop(2, PIECES)
         def _(j):
-            give_in(b2, 0, j)
+            give_in(2, 0, j)
 
         @pl.loop(0, PIECES)
         def _(j):
-            give_in(b3, 0, j)
+            give_in(3, 0, j)
 
         settle()
 
         @pl.loop(0, PIECES)
         def _(j):
             give_out(0, j)
-            give_in(b3, 1, j)
-
-        give_out(1, 0)
-        give_out(1, 1)
+            give_in(3, 1, j)
+
+        @pl.loop(0, 2)
+        def _(j):
+            give_out(1, j)
 
         @pl.loop(2, PIECES)
         def _(j):
-            give_in(b2, 1, j)
+            give_in(2, 1, j)
             give_out(1, j)
-
-        for r in range(HALVES + 1):
-            for b in (own, b0):
-                mid_in(b, r).wait_send()
-            for b in (own, b2, b3):
-                mid_out(b, r).wait_send()
-
-        @pl.loop(0, PIECES)
-        def _(j):
-            mid_give_in(b2, 0, j).wait_send()
-            mid_give_in(b3, 0, j).wait_send()
-            mid_give_in(b3, 1, j).wait_send()
 
         for r in range(HALVES):
 
             @pl.loop(0, PIECES)
             def _(j):
-                sum_in(own, r, j)
-                sum_out(own, r, j)
+                sum_in(1, r, j)
+                sum_out(1, r, j)
 
             total = (
                 branch[half(r)]
@@ -748,11 +757,8 @@
             )
             yield_out(r, total)
 
-        @pl.loop(0, PIECES)
-        def _(j):
-            mid_give_in(b2, 1, j).wait_send()
-            for r in range(HALVES):
-                mid_give_out(b0, r, j).wait_send()
+        drain(in_send, e_recv, 2 * sent_block + 2 * sent_sums).wait_send()
+        drain(out_send, e_recv, 3 * sent_block + sent_sums).wait_send()
 
     for r in range(HALVES):
         out_copy(r).wait()
@@ -818,18 +824,22 @@
             pltpu.VMEM((rows, width), bf),
             dma((17,)),
             dma((HALVES,)),
-            dma((2,)),
-            dma((2,)),
-            dma((1,)),
-            dma((1,)),
-            dma((2,)),
+        ]
+        + [dma((1,))] * 6
+        + [
             dma((2,)),
             dma((PIECES,)),
-            dma((PIECES,)),
-        ]
-        + [dma((count,))] * 8
-        + [dma((line, HALVES + 1))] * 4
-        + [dma((line, HALVES, PIECES))] * 4,
+            dma((2, 2)),
+            dma((PIECES + 1,)),
+            dma((count,)),
+            dma((1 + PIECES,)),
+            dma((count,)),
+            dma((1 + PIECES,)),
+            dma((line - 1, HALVES + 1)),
+            dma((HALVES + 1,)),
+            dma((2, HALVES, PIECES)),
+            dma((line - 1, HALVES, PIECES)),
+        ],
         compiler_params=pltpu.CompilerParams(
             collective_id=0, has_side_effects=True, vmem_limit_bytes=60 * 1024 * 1024
         ),

time: 85.1 us -> 83.2 us (0.978)
  Pallas kernels: 83.1 us -> 81.2 us
    pallas_call x1, Pallas kernels: 83.1 us -> 81.2 us  [fused_layer(): pl.pallas_call(functools.partial(layer_kernel, line), out_shape=jax.Shape...]
where the time goes in v4:
time: 83.2 us; the launch traced here: 83.1 us
  Pallas kernels  81.2 us (98%)
  local copies, waits for them, and re-layouts  1.88 us (2%)
    pallas_call x1, Pallas kernels, fused_layer(): pl.pallas_call(functools.partial(layer_kernel, line), out_shape=jax.Shape...  81.2 us
    unnamed x1, local copies, waits for them, and re-layouts  1.88 us

profile of v4, /device:TPU:0, one launch (start us, length us, event | category | flops | bytes accessed | tf_op | source)
XLA Modules:
  0.0 83.1 jit_solution(6544956328242387785)
XLA Ops:
  0.0 81.2 %shard_map.163 = bf16[128,2048]{1,0:T(8,128)(2,1)} custom-call(bf16[512,256]{1,0:T(8,128)(2,1)} %x_hbm.1, bf16[512,256]{1,0:T(8,128)(2,1)} %gate_b_hbm.1, bf16[512,256]{1,0:T(8,128)(2,1)} %gate_c_hbm.1, bf16[3,256]{1,0:T(4,128)(2,1)} %taps_hbm.1, bf16[128,2048]{1,0:T(8,128)(2,1)} %resid_hbm.1, bf16[2048]{0:T(1024)(128)(2,1)} %mix_hbm.1, ...), custom_call_target="tpu_custom_call" | custom-call | tf_op jit(solution)/shard_map/pallas_call | solution.py:784
  81.2 1.9 %copy.19 = bf16[128,2048]{1,0:T(8,128)(2,1)} copy(bf16[128,2048]{1,0:T(8,128)(2,1)} %shard_map.163) | data formatting | bytes 1048576

commit v5 on v4

--- a/solution.py
+++ b/solution.py
@@ -11,8 +11,9 @@
 epsilon = 1e-06
 PIECES = 4
 HALVES = 2
-DIRECT = (3, 7)
-ORDER = (0, 1, 2, 3, 4, -3, 5, 6, 7, -7)
+DIRECT = (4, 5, 8)
+ORDER = (0, 1, 2, 3, 4, -4, 6, 5, -5, 7, 8, -8)
+CUTS = ((0, 0, 2), (0, 2, 2), (1, 0, 2), (1, 2, 1), (1, 3, 1))
 TABLE = HALVES
 
 
@@ -231,25 +232,22 @@
         device_id_type=MESH,
     )
 
-    pieces = []
-    for ref, held in ((eg_ref, w_gate), (eu_ref, w_up)):
-        for h in range(HALVES):
-            pieces.append((ref, held, h))
+    pieces = [((eg_ref, w_gate), (eu_ref, w_up))[k] + (first, size) for k, first, size in CUTS]
     for j in range(PIECES):
-        pieces.append((ed_ref, w_down, j))
+        pieces.append((ed_ref, w_down, j, 1))
     count = len(pieces)
 
     def cut(n, owner):
-        ref, held, h = pieces[n]
+        ref, held, first, steps = pieces[n]
         if held is w_down:
             size = hid // tp_size
             begin = pl.multiple_of(owner * size, size)
             return (
-                ref.at[0, pl.ds(begin, size), chunk(h)],
-                held.at[pl.ds(pl.multiple_of(hid + begin, size), size), chunk(h)],
+                ref.at[0, pl.ds(begin, size), chunk(first)],
+                held.at[pl.ds(pl.multiple_of(hid + begin, size), size), chunk(first)],
             )
-        size = ref.shape[1] // tp_size // HALVES
-        where = pl.ds(pl.multiple_of((owner * HALVES + h) * size, size), size)
+        size = ref.shape[1] // tp_size // 4
+        where = pl.ds(pl.multiple_of((owner * 4 + first) * size, size), size * steps)
         return ref.at[0, where], held.at[1, where]
 
     def hop(n, owner, target, send, recv, first=False):
@@ -264,7 +262,7 @@
         )
 
     def late(n):
-        return max(0, n - 2 * HALVES + 1)
+        return min(n // 2, 1) + max(0, n - len(CUTS) + 1)
 
     def x_hop(n):
         return hop(n, tp, (mate, tp), spread_send, wx_recv.at[n], True)
@@ -309,11 +307,10 @@
             near_hop(n, near).wait_recv()
             relay_hop(n, near_far).wait_recv()
 
-    def ready_both():
-        size = 2 * hid // tp_size
+    def ready_part(k):
         with jax.named_scope("w_ready"):
-            drain(spread_send, wn_recv, size).wait_recv()
-            drain(relay_send, wr_recv, size).wait_recv()
+            drain(spread_send, wn_recv.at[pl.ds(k, 1)], hid // tp_size).wait_recv()
+            drain(relay_send, wr_recv.at[pl.ds(k, 1)], hid // tp_size).wait_recv()
 
     def block_copy(b, r, target, send, recv):
         ref = shares.at[b] if r == TABLE else blocks.at[b, half(r)]
@@ -422,7 +419,8 @@
 
         @pl.when(level == 1)
         def _():
-            mid_in(1, r).start()
+            if r != HALVES - 1:
+                mid_in(1, r).start()
             mid_out(1, r).start()
 
     send_own(TABLE)
@@ -512,13 +510,38 @@
             jnp.where(lanes[:size] == expert, shares[b, part], 0.0), axis=1, keepdims=True
         )
 
-        @pl.loop(0, hid // 256)
-        def _(j):
+        def step(j):
             cols = pl.ds(pl.multiple_of(j * 256, 256), 256)
             gate = jnp.dot(blocks[b, part], w_gate[e, :, cols], preferred_element_type=jnp.float32)
             up = jnp.dot(blocks[b, part], w_up[e, :, cols], preferred_element_type=jnp.float32)
             kept = pl.ds(pl.multiple_of(e * hid + j * 256, 256), 256)
             hidden[b, part, kept] = (jax.nn.silu(gate) * up * share).astype(jnp.bfloat16)
+
+        if size < rows:
+            for j in range(hid // 256):
+                step(j)
+        else:
+            pl.loop(0, hid // 256)(step)
+
+    def share_of(b, e):
+        expert = z * 2 + x + e * (1 - 2 * x)
+        return jnp.sum(jnp.where(lanes == expert, shares[b], 0.0), axis=1, keepdims=True)
+
+    def gate_ahead(b):
+        share = share_of(b, 1)
+
+        @pl.loop(0, hid // 256)
+        def _(j):
+            cols = pl.ds(pl.multiple_of(j * 256, 256), 256)
+            gate = jnp.dot(blocks[b], w_gate[1, :, cols], preferred_element_type=jnp.float32)
+            projected[:, cols] = jax.nn.silu(gate) * share
+
+    def up_after(b):
+        for j in range(hid // 256):
+            cols = pl.ds(j * 256, 256)
+            up = jnp.dot(blocks[b], w_up[1, :, cols], preferred_element_type=jnp.float32)
+            kept = pl.ds(hid + j * 256, 256)
+            hidden[b, :, kept] = (projected[:, cols] * up).astype(jnp.bfloat16)
 
     def hide_all(b, e):
         hide(b, 0, rows, e)
@@ -590,55 +613,68 @@
         hide(rel(1), 0, half_rows, 0)
         spread(4)
         relay(1)
+        relay(4)
+        spread(6)
         got_in(1, 1)
         hide(rel(1), half_rows, half_rows, 0)
         relay(2)
+        ready_part(0)
+        gate_ahead(rel(1))
+        spread(5)
         relay(3)
-        ready_both()
-        hide_all(rel(1), 1)
-        relay(4)
-        spread(5)
-        ready(4)
+        relay(5)
+        ready_part(1)
+        up_after(rel(1))
+        ready(5)
         for r in range(HALVES):
             give(1, r, 0, None, edge_give)
-        spread(6)
+        relay(6)
+        spread(7)
+        ready(6)
+        for r in range(HALVES):
+            give(1, r, 1, None, edge_give)
         got_in(2, TABLE)
         got_in(2, 0)
         hide_half(rel(2), 0)
-        give(2, 0, 0, None, edge_give)
-        relay(5)
-        spread(7)
-        ready(5)
-        for r in range(HALVES):
-            give(1, r, 1, None, edge_give)
-        give(2, 0, 1, None, edge_give)
-        relay(6)
+
+        @pl.loop(0, 2)
+        def _(j):
+            give(2, 0, j, None, edge_give)
+
+        spread(8)
+        got_in(3, TABLE)
+        got_in(3, 0)
+        hide_half(rel(3), 0)
+
+        @pl.loop(0, 2)
+        def _(j):
+            give(3, 0, j, None, edge_give)
+
         relay(7)
+        relay(8)
+        ready(7)
+        ready(8)
+
+        @pl.loop(2, PIECES)
+        def _(j):
+            give(3, 0, j, None, edge_give)
+
+        got_in(3, 1)
+        hide_half(rel(3), 1)
+
+        @pl.loop(0, PIECES)
+        def _(j):
+            give(3, 1, j, None, edge_give)
+
+        @pl.loop(2, PIECES)
+        def _(j):
+            give(2, 0, j, None, edge_give)
+
+        hide_all(own, 1)
         got_in(2, 1)
         hide_half(rel(2), 1)
 
-        @pl.loop(0, 2)
-        def _(j):
-            give(2, 1, j, None, edge_give)
-
-        ready(6)
-        ready(7)
-
-        @pl.loop(2, PIECES)
-        def _(j):
-            give(2, 0, j, None, edge_give)
-
-        hide_all(own, 1)
-        got_in(3, TABLE)
-        for r in range(HALVES):
-            got_in(3, r)
-            hide_half(rel(3), r)
-
-            @pl.loop(0, PIECES)
-            def _(j):
-                give(3, r, j, None, edge_give)
-
-        @pl.loop(2, PIECES)
+        @pl.loop(0, PIECES)
         def _(j):
             give(2, 1, j, None, edge_give)
 
@@ -677,28 +713,32 @@
         pass_out(3, TABLE)
         spread(4)
         relay(1)
+        relay(4)
+        spread(6)
         pass_in(1)
-        pass_out(2, 1)
+        mid_in(1, HALVES - 1).start()
+        pass_out(3, 0)
         hide_all(rel(0), 0)
         relay(2)
+        spread(5)
         relay(3)
-        hide_all(rel(2), 0)
-        relay(4)
-        spread(5)
-        ready_both()
-        pass_out(3, 0)
-        hide_all(rel(2), 1)
-        spread(6)
         relay(5)
+        ready_part(0)
+        ready_part(1)
+        hide_half(rel(2), 0)
+        relay(6)
         spread(7)
+        pass_out(3, 1)
         hide_all(own, 1)
-        pass_out(3, 1)
-        relay(6)
+        spread(8)
+        hide_all(rel(3), 0)
         relay(7)
-        hide_all(rel(3), 0)
+        relay(8)
         hide_all(rel(3), 1)
+        pass_out(2, 1)
+        hide_half(rel(2), 1)
         hide_all(rel(0), 1)
-        for n in range(4, count):
+        for n in range(len(CUTS), count):
             ready(n)
 
         def give_in(k, r, j):
@@ -715,14 +755,6 @@
 
         own_branch()
 
-        @pl.loop(0, 2)
-        def _(j):
-            give_in(2, 1, j)
-
-        @pl.loop(2, PIECES)
-        def _(j):
-            give_in(2, 0, j)
-
         @pl.loop(0, PIECES)
         def _(j):
             give_in(3, 0, j)
@@ -740,8 +772,12 @@
 
         @pl.loop(2, PIECES)
         def _(j):
+            give_in(2, 0, j)
+            give_out(1, j)
+
+        @pl.loop(0, PIECES)
+        def _(j):
             give_in(2, 1, j)
-            give_out(1, j)
 
         for r in range(HALVES):
 
@@ -775,7 +811,7 @@
     hid = expert_gate.shape[2]
     shared_hid = shared_gate.shape[1]
     dma = pltpu.SemaphoreType.DMA
-    count = 2 * HALVES + PIECES
+    count = len(CUTS) + PIECES
     bf, f32 = jnp.bfloat16, jnp.float32
     hbm = pl.BlockSpec(memory_space=pltpu.HBM)
     lanes = 128 * (-(-experts // 128))
@@ -832,9 +868,9 @@
             dma((2, 2)),
             dma((PIECES + 1,)),
             dma((count,)),
-            dma((1 + PIECES,)),
+            dma((2 + PIECES,)),
             dma((count,)),
-            dma((1 + PIECES,)),
+            dma((2 + PIECES,)),
             dma((line - 1, HALVES + 1)),
             dma((HALVES + 1,)),
             dma((2, HALVES, PIECES)),

time: 83.2 us -> 80.5 us (0.968)
  the two profiles are of different devices: /device:TPU:0 before, /device:TPU:17 now
where the time goes in v5:
time: 80.5 us; the launch traced here: 80.3 us
  Pallas kernels  78.5 us (98%)
  local copies, waits for them, and re-layouts  1.88 us (2%)
    pallas_call x1, Pallas kernels, fused_layer(): pl.pallas_call(functools.partial(layer_kernel, line), out_shape=jax.Shape...  78.5 us
    unnamed x1, local copies, waits for them, and re-layouts  1.88 us

profile of v5, /device:TPU:17, one launch (start us, length us, event | category | flops | bytes accessed | tf_op | source)
XLA Modules:
  0.0 80.3 jit_solution(13390634290511204001)
XLA Ops:
  0.0 78.5 %shard_map.163 = bf16[128,2048]{1,0:T(8,128)(2,1)} custom-call(bf16[512,256]{1,0:T(8,128)(2,1)} %x_hbm.1, bf16[512,256]{1,0:T(8,128)(2,1)} %gate_b_hbm.1, bf16[512,256]{1,0:T(8,128)(2,1)} %gate_c_hbm.1, bf16[3,256]{1,0:T(4,128)(2,1)} %taps_hbm.1, bf16[128,2048]{1,0:T(8,128)(2,1)} %resid_hbm.1, bf16[2048]{0:T(1024)(128)(2,1)} %mix_hbm.1, ...), custom_call_target="tpu_custom_call" | custom-call | tf_op jit(solution)/shard_map/pallas_call | solution.py:820
  78.5 1.9 %copy.19 = bf16[128,2048]{1,0:T(8,128)(2,1)} copy(bf16[128,2048]{1,0:T(8,128)(2,1)} %shard_map.163) | data formatting | bytes 1048576

commit v6 on v5

--- a/solution.py
+++ b/solution.py
@@ -71,9 +71,7 @@
     outgoing,
     from_out,
     from_in,
-    out_v,
     load_sem,
-    out_sem,
     edge_send,
     misc_send,
     spread_send,
@@ -383,10 +381,6 @@
         else:
             x_hop(n).start()
 
-    loads[2].wait()
-    for j in range(PIECES):
-        proj_copy(j).start()
-
     for n in (0, 1, 3, 4):
         loads[n].wait()
     mixed[:pad] = jnp.zeros((pad, channels), jnp.float32)
@@ -401,6 +395,9 @@
 
     convolve(all_rows)
     conv_copy(1, 0).start()
+    loads[2].wait()
+    for j in range(PIECES):
+        proj_copy(j).start()
     conv_copy(0, 0).start()
     loads[5].wait()
     loads[6].wait()
@@ -574,16 +571,12 @@
                 shared_hidden[...], s_down[:, chunk(j)], preferred_element_type=jnp.float32
             )
 
-    def out_copy(r):
-        return pltpu.make_async_copy(out_v.at[half(r)], out_ref.at[half(r)], out_sem.at[r])
-
     def yield_out(r, total):
         factor = lax.rsqrt(jnp.mean(total * total, axis=1, keepdims=True) + epsilon)
-        out_v[half(r)] = (
+        out_ref[half(r)] = (
             resid1[half(r)].astype(jnp.float32)
             + total * factor * post_ref[...].astype(jnp.float32).reshape(1, width)
         ).astype(jnp.bfloat16)
-        out_copy(r).start()
 
     def settle():
         @pl.when(sp < sp_size - 1)
@@ -796,9 +789,6 @@
         drain(in_send, e_recv, 2 * sent_block + 2 * sent_sums).wait_send()
         drain(out_send, e_recv, 3 * sent_block + sent_sums).wait_send()
 
-    for r in range(HALVES):
-        out_copy(r).wait()
-
 
 def fused_layer(
     x_in, gate_b, gate_c, conv_taps, out_proj, mix_gain, resid, pre_gain, expert_gate, expert_up,
@@ -821,7 +811,7 @@
         functools.partial(layer_kernel, line),
         out_shape=jax.ShapeDtypeStruct((rows, width), bf),
         in_specs=[hbm] * 17,
-        out_specs=hbm,
+        out_specs=pl.BlockSpec(memory_space=pltpu.VMEM),
         scratch_shapes=[
             pltpu.VMEM((all_rows, channels), bf),
             pltpu.VMEM((all_rows, channels), bf),
@@ -857,9 +847,7 @@
             pltpu.VMEM((line, rows, width), bf),
             pltpu.VMEM((line, rows, width), bf),
             pltpu.VMEM((line, rows, width), bf),
-            pltpu.VMEM((rows, width), bf),
             dma((17,)),
-            dma((HALVES,)),
         ]
         + [dma((1,))] * 6
         + [
@@ -877,12 +865,17 @@
             dma((line - 1, HALVES, PIECES)),
         ],
         compiler_params=pltpu.CompilerParams(
-            collective_id=0, has_side_effects=True, vmem_limit_bytes=60 * 1024 * 1024
+            collective_id=0, has_side_effects=True, vmem_limit_bytes=46 * 1024 * 1024
         ),
     )(
-        x_in, gate_b, gate_c, conv_taps, resid, mix_gain, pre_gain, post_gain,
-        routes.T, route_weights.T, out_proj, expert_gate, expert_up, expert_down,
-        shared_gate, shared_up, shared_down,
+        *(
+            pltpu.with_memory_space_constraint(ref, pltpu.HBM)
+            for ref in (
+                x_in, gate_b, gate_c, conv_taps, resid, mix_gain, pre_gain, post_gain,
+                routes.T, route_weights.T, out_proj, expert_gate, expert_up, expert_down,
+                shared_gate, shared_up, shared_down,
+            )
+        )
     )
 
 

time: 80.5 us -> 78.5 us (0.975)
  the two profiles are of different devices: /device:TPU:17 before, /device:TPU:0 now
where the time goes in v6:
time: 78.5 us; the launch traced here: 77.4 us
  Pallas kernels  76.6 us (98%)
  local copies, waits for them, and re-layouts  0.8 us (1%)
    pallas_call x1, Pallas kernels, fused_layer(): pl.pallas_call(functools.partial(layer_kernel, line), out_shape=jax.Shape...  76.6 us

profile of v6, /device:TPU:0, one launch (start us, length us, event | category | flops | bytes accessed | tf_op | source)
XLA Modules:
  0.0 77.4 jit_solution(11137777036089912269)
XLA Ops:
  0.0 76.6 %shard_map.163 = bf16[128,2048]{1,0:T(8,128)(2,1)S(1)} custom-call(bf16[512,256]{1,0:T(8,128)(2,1)} %x_hbm.1, bf16[512,256]{1,0:T(8,128)(2,1)} %gate_b_hbm.1, bf16[512,256]{1,0:T(8,128)(2,1)} %gate_c_hbm.1, bf16[3,256]{1,0:T(4,128)(2,1)} %taps_hbm.1, bf16[128,2048]{1,0:T(8,128)(2,1)} %resid_hbm.1, bf16[2048]{0:T(1024)(128)(2,1)} %mix_hbm.1, ...), custom_call_target="tpu_custom_call" | custom-call | tf_op jit(solution)/shard_map/pallas_call | solution.py:810
  76.6 0.8 %copy.19 = bf16[128,2048]{1,0:T(8,128)(2,1)} copy(bf16[128,2048]{1,0:T(8,128)(2,1)S(1)} %shard_map.163) | data formatting | bytes 1048576

commit v7 on v6

--- a/solution.py
+++ b/solution.py
@@ -13,7 +13,8 @@
 HALVES = 2
 DIRECT = (4, 5, 8)
 ORDER = (0, 1, 2, 3, 4, -4, 6, 5, -5, 7, 8, -8)
-CUTS = ((0, 0, 2), (0, 2, 2), (1, 0, 2), (1, 2, 1), (1, 3, 1))
+CUTS = ((0, 0, 8), (0, 8, 8), (1, 0, 8), (1, 8, 5), (1, 13, 3))
+SLICES = 16
 TABLE = HALVES
 
 
@@ -244,8 +245,8 @@
                 ref.at[0, pl.ds(begin, size), chunk(first)],
                 held.at[pl.ds(pl.multiple_of(hid + begin, size), size), chunk(first)],
             )
-        size = ref.shape[1] // tp_size // 4
-        where = pl.ds(pl.multiple_of((owner * 4 + first) * size, size), size * steps)
+        size = ref.shape[1] // tp_size // SLICES
+        where = pl.ds(pl.multiple_of((owner * SLICES + first) * size, size), size * steps)
         return ref.at[0, where], held.at[1, where]
 
     def hop(n, owner, target, send, recv, first=False):
@@ -635,6 +636,8 @@
             give(2, 0, j, None, edge_give)
 
         spread(8)
+        relay(7)
+        relay(8)
         got_in(3, TABLE)
         got_in(3, 0)
         hide_half(rel(3), 0)
@@ -643,8 +646,6 @@
         def _(j):
             give(3, 0, j, None, edge_give)
 
-        relay(7)
-        relay(8)
         ready(7)
         ready(8)
 

time: 78.5 us -> 78.3 us (level)
  no operation moved by 1% of the time
where the time goes in v7:
time: 78.3 us; the launch traced here: 77.2 us
  Pallas kernels  76.4 us (98%)
  local copies, waits for them, and re-layouts  0.8 us (1%)
    pallas_call x1, Pallas kernels, fused_layer(): pl.pallas_call(functools.partial(layer_kernel, line), out_shape=jax.Shape...  76.4 us

profile of v7, /device:TPU:0, one launch (start us, length us, event | category | flops | bytes accessed | tf_op | source)
XLA Modules:
  0.0 77.2 jit_solution(9404599663921005868)
XLA Ops:
  0.0 76.4 %shard_map.163 = bf16[128,2048]{1,0:T(8,128)(2,1)S(1)} custom-call(bf16[512,256]{1,0:T(8,128)(2,1)} %x_hbm.1, bf16[512,256]{1,0:T(8,128)(2,1)} %gate_b_hbm.1, bf16[512,256]{1,0:T(8,128)(2,1)} %gate_c_hbm.1, bf16[3,256]{1,0:T(4,128)(2,1)} %taps_hbm.1, bf16[128,2048]{1,0:T(8,128)(2,1)} %resid_hbm.1, bf16[2048]{0:T(1024)(128)(2,1)} %mix_hbm.1, ...), custom_call_target="tpu_custom_call" | custom-call | tf_op jit(solution)/shard_map/pallas_call | solution.py:811
  76.4 0.8 %copy.19 = bf16[128,2048]{1,0:T(8,128)(2,1)} copy(bf16[128,2048]{1,0:T(8,128)(2,1)S(1)} %shard_map.163) | data formatting | bytes 1048576

commit v8 on v7

--- a/solution.py
+++ b/solution.py
@@ -553,9 +553,10 @@
             hidden[b, part], w_down[:, chunk(j)], preferred_element_type=jnp.float32
         )
 
-    def give(k, r, j, arrived, send):
+    def give(k, r, j, arrived, send, landed=None):
         made = down(rel(k), half(r), j)
         if arrived is not None:
+            landed(k, r, j)
             made += arrived[rel(k), half(r), chunk(j)].astype(jnp.float32)
         outgoing[rel(k), half(r), chunk(j)] = made.astype(jnp.bfloat16)
         send(k, r, j).start()
@@ -736,12 +737,10 @@
             ready(n)
 
         def give_in(k, r, j):
-            sum_out(k, r, j)
-            give(k, r, j, from_out, mid_give_in)
+            give(k, r, j, from_out, mid_give_in, sum_out)
 
         def give_out(r, j):
-            sum_in(0, r, j)
-            give(0, r, j, from_in, mid_give_out)
+            give(0, r, j, from_in, mid_give_out, sum_in)
 
         @pl.loop(0, 2)
         def _(j):

time: 78.3 us -> 78.3 us (level)
  no operation moved by 1% of the time
where the time goes in v8:
time: 78.3 us; the launch traced here: 77.2 us
  Pallas kernels  76.4 us (98%)
  local copies, waits for them, and re-layouts  0.8 us (1%)
    pallas_call x1, Pallas kernels, fused_layer(): pl.pallas_call(functools.partial(layer_kernel, line), out_shape=jax.Shape...  76.4 us

profile of v8, /device:TPU:0, one launch (start us, length us, event | category | flops | bytes accessed | tf_op | source)
XLA Modules:
  0.0 77.2 jit_solution(11727580078935906195)
XLA Ops:
  0.0 76.4 %shard_map.163 = bf16[128,2048]{1,0:T(8,128)(2,1)S(1)} custom-call(bf16[512,256]{1,0:T(8,128)(2,1)} %x_hbm.1, bf16[512,256]{1,0:T(8,128)(2,1)} %gate_b_hbm.1, bf16[512,256]{1,0:T(8,128)(2,1)} %gate_c_hbm.1, bf16[3,256]{1,0:T(4,128)(2,1)} %taps_hbm.1, bf16[128,2048]{1,0:T(8,128)(2,1)} %resid_hbm.1, bf16[2048]{0:T(1024)(128)(2,1)} %mix_hbm.1, ...), custom_call_target="tpu_custom_call" | custom-call | tf_op jit(solution)/shard_map/pallas_call | solution.py:810
  76.4 0.8 %copy.19 = bf16[128,2048]{1,0:T(8,128)(2,1)} copy(bf16[128,2048]{1,0:T(8,128)(2,1)S(1)} %shard_map.163) | data formatting | bytes 1048576
